TPU v7x, 128 devices: a whole 4x4x4 slice. The times are simulated.
128 devices in a mesh: sp: 32 (over z, y, core), tp: 4 (over x).
Axes of the slice: x: 4, y: 4, z: 4, core: 2. Of those that a mesh axis runs over, the one named last changes fastest.
Arguments:
- inputs: bfloat16 [49152, 2048], P('sp'), may hold values from -6 to 6
- norm_gain: float32 [2048], replicated, may hold values from 0.1 to 1.9
- pool_weight: bfloat16 [2048, 1024], P(None, 'tp'), may hold values from -0.125 to 0.125
- query_weight: bfloat16 [2048, 1024], P(None, 'tp'), may hold values from -0.125 to 0.125
- forget_weight: bfloat16 [2048, 1024], P(None, 'tp'), may hold values from -0.125 to 0.125
- value_weight: bfloat16 [2048, 1024], P(None, 'tp'), may hold values from -0.125 to 0.125
- outgate_weight: bfloat16 [2048, 1024], P(None, 'tp'), may hold values from -0.125 to 0.125
- pool_mix: bfloat16 [4, 256, 256], P('tp'), may hold values from -0.375 to 0.375
- pool_scale: float32 [1024], P('tp'), may hold values from 0.1 to 1.9
- lower_bound: float32 [1024], P('tp'), may hold values from 0.9 to 1
- extra_decay: float32 [49152, 8], P('sp', 'tp'), may hold values from -1 to 0
- recur_gain: float32 [1024], P('tp'), may hold values from 0.1 to 1.9
- init_state: float32 [8, 128, 128], P('tp'), may hold values from -0.0067658233 to 0.0067658233
- out_pool: bfloat16 [1024, 2048], P('tp'), may hold values from -0.125 to 0.125
- out_recur: bfloat16 [1024, 2048], P('tp'), may hold values from -0.125 to 0.125
Outputs:
- mixed: bfloat16 [49152, 2048], P(('sp', 'tp'))
All inputs are finite; a program needn't handle non-finite values.
Results may differ from a plain program's by a relative error of at most 0.014.
Values may be sent and summed in bfloat16 or wider, within the bound.
A program may use at most 128 MiB of HBM per device.

v0:
```python
import jax
import jax.numpy as jnp
from jax import lax
from jax.sharding import Mesh
from jax.sharding import PartitionSpec as P

GROUPS = 4
BLOCK = 64
SP = ("sp_0", "sp_1", "sp_2")
SP_TP = ("sp_0", "sp_1", "sp_2", "tp")


norm_eps = 1e-05
halo_rows = 16


def shifted_2(array, axis, by):
    devices = lax.axis_size(axis)
    pairs = [(i, i + by) for i in range(devices) if 0 <= i + by < devices]
    return lax.ppermute(array, axis, pairs)


def neutral_like(array, identity):
    return jax.tree.map(
        lambda part, zero: jnp.zeros_like(part) + jnp.asarray(zero, part.dtype), array, identity
    )


def prefix_by_axis(array, axes, combine, identity):
    before = start = neutral_like(array, identity)
    subtotal = array
    for axis in reversed(axes):
        devices, index = (lax.axis_size(axis), lax.axis_index(axis))
        pieces = jax.tree.map(lambda part: lax.all_gather(part, axis), subtotal)
        inside, subtotal = (start, start)
        for k in range(devices):
            passed = k < index
            subtotal = combine(subtotal, jax.tree.map(lambda part: part[k], pieces))
            inside = jax.tree.map(lambda new, old: jnp.where(passed, new, old), subtotal, inside)
        before = combine(inside, before)
    return before


def sent_together(arrays, axis, dim, along):
    ends, at = ([], 0)
    for a in arrays[:-1]:
        at += a.shape[along]
        ends.append(at)
    both = jnp.concatenate(arrays, axis=along)
    return tuple(jnp.split(lax.all_gather(both, axis, axis=dim, tiled=True), ends, axis=along))


def norm_rows(array, scale_vec):
    widened = array.astype(jnp.float32)
    scaled = widened * lax.rsqrt(jnp.mean(widened * widened, axis=-1, keepdims=True) + norm_eps)
    return (scaled * scale_vec).astype(jnp.bfloat16)


def window_sums(widened):
    results = []
    current = widened
    for level_idx in range(GROUPS):
        stride = 2**level_idx
        shifted = jnp.pad(current, ((stride, 0), (0, 0)))[: current.shape[0]]
        current = current + shifted
        results.append(current)
    return results


def pool_branch(pool_in, earlier, pool_mix, pool_scale, first_pos, group_first):
    row_count = pool_in.shape[0]
    group_width = pool_mix.shape[1]
    margin = earlier.shape[0]
    widened = jnp.concatenate([earlier.astype(jnp.float32), pool_in.astype(jnp.float32)], axis=0)
    window_totals = window_sums(widened)
    token_positions = first_pos + jnp.arange(row_count, dtype=jnp.int32)
    group_idx = group_first + 0
    columns = slice(0, group_width)
    picked = jnp.zeros((row_count, group_width), jnp.float32)
    counted = jnp.ones((row_count,), jnp.float32)
    for level_idx in range(GROUPS):
        chosen = group_idx == level_idx
        picked = jnp.where(chosen, window_totals[level_idx][margin:, columns], picked)
        reach = jnp.minimum(token_positions + 1, 2 ** (level_idx + 1)).astype(jnp.float32)
        counted = jnp.where(chosen, reach, counted)
    pieces = [picked / counted[:, None] - widened[margin:, columns]]
    pooled = jnp.stack(pieces, axis=1).astype(jnp.bfloat16)
    mixed_groups = jnp.einsum("rgc,gcd->rgd", pooled, pool_mix, preferred_element_type=jnp.float32)
    return (mixed_groups.reshape(row_count, -1) * pool_scale).astype(jnp.bfloat16)


def recur_inputs(query_raw, forget_raw, value_raw, bound_vec, extra_log, head_k, block_len):
    row_count = query_raw.shape[0]
    count_of_heads = query_raw.shape[1] // head_k
    block_count = row_count // block_len
    forget_pre = forget_raw.astype(jnp.float32)
    log_f = jnp.logaddexp(
        jnp.log(bound_vec), jnp.log1p(-bound_vec) + jax.nn.log_sigmoid(forget_pre)
    )
    log_f = log_f.reshape(row_count, count_of_heads, head_k) + extra_log[:, :, None]
    key_input = ((1.0 - bound_vec) * jax.nn.sigmoid(-forget_pre)).reshape(
        row_count, count_of_heads, head_k
    )
    query_input = jax.nn.silu(query_raw.astype(jnp.float32)).reshape(
        row_count, count_of_heads, head_k
    )
    value_input = value_raw.astype(jnp.float32).reshape(row_count, count_of_heads, head_k)

    def to_blocks(array):
        return array.reshape(block_count, block_len, count_of_heads, head_k).transpose(2, 0, 1, 3)

    return (to_blocks(query_input), to_blocks(key_input), to_blocks(value_input), to_blocks(log_f))


def block_parts(query_input, key_input, value_input, log_f):
    block_len = log_f.shape[2]
    cum_log = jnp.cumsum(log_f, axis=2)
    last_log = cum_log[:, :, -1:, :]
    query_dec = query_input * jnp.exp(cum_log)
    key_dec = key_input * jnp.exp(-cum_log)
    scores = jnp.einsum("hntk,hnsk->hnts", query_dec, key_dec)
    causal = jnp.tril(jnp.ones((block_len, block_len), dtype=bool))
    scores = jnp.where(causal, scores, 0.0)
    within = jnp.einsum("hnts,hnsv->hntv", scores, value_input)
    contrib = jnp.einsum("hnsk,hnsv->hnkv", key_input * jnp.exp(last_log - cum_log), value_input)
    decays = jnp.exp(last_log[:, :, 0, :])
    return (query_dec, within, decays, contrib)


def chain(earlier, later_part):
    return (earlier[0] * later_part[0], later_part[0][..., None] * earlier[1] + later_part[1])


def per_device(
    inputs,
    norm_gain,
    pool_weight,
    query_weight,
    forget_weight,
    value_weight,
    outgate_weight,
    pool_mix,
    pool_scale,
    lower_bound,
    extra_decay,
    recur_gain,
    init_state,
    out_pool,
    out_recur,
):
    row_count = inputs.shape[0]
    count_of_heads = init_state.shape[0]
    head_k = init_state.shape[1]
    normed = norm_rows(inputs, norm_gain)
    pool_in = jnp.dot(normed, pool_weight, preferred_element_type=jnp.float32).astype(jnp.bfloat16)
    query_raw = jnp.dot(normed, query_weight, preferred_element_type=jnp.float32).astype(
        jnp.bfloat16
    )
    forget_raw = jnp.dot(normed, forget_weight, preferred_element_type=jnp.float32).astype(
        jnp.bfloat16
    )
    value_raw = jnp.dot(normed, value_weight, preferred_element_type=jnp.float32).astype(
        jnp.bfloat16
    )
    outgate_raw = jnp.dot(normed, outgate_weight, preferred_element_type=jnp.float32).astype(
        jnp.bfloat16
    )
    tail_part = pool_in[row_count - halo_rows :]
    query_in, key_in, value_in, log_f = recur_inputs(
        query_raw, forget_raw, value_raw, lower_bound, extra_decay, head_k, BLOCK
    )
    query_dec, within, decays, contrib = block_parts(query_in, key_in, value_in, log_f)
    running = lax.associative_scan(chain, (decays, contrib), axis=1)
    totals_a = running[0][:, -1]
    totals_s = running[1][:, -1]
    unit_decay = jnp.ones_like(totals_a)
    zero_state = jnp.zeros_like(totals_s)
    earlier = shifted_2(tail_part, SP, 1)
    prior_decay, prior_state = prefix_by_axis(
        (totals_a, totals_s), SP, chain, (unit_decay, zero_state)
    )
    first_pos = lax.axis_index(SP) * row_count
    group_first = lax.axis_index("tp") * pool_mix.shape[0]
    y_pool = pool_branch(pool_in, earlier, pool_mix, pool_scale, first_pos, group_first)
    carried = prior_state + prior_decay[..., None] * init_state
    enter_a = jnp.concatenate([jnp.ones_like(decays[:, :1]), running[0][:, :-1]], axis=1)
    enter_s = jnp.concatenate([jnp.zeros_like(contrib[:, :1]), running[1][:, :-1]], axis=1)
    state_in = enter_s + enter_a[..., None] * carried[:, None]
    recur_out = within + jnp.einsum("hntk,hnkv->hntv", query_dec, state_in)
    recur_out = recur_out.transpose(1, 2, 0, 3).reshape(row_count, count_of_heads, head_k)
    recur_out = recur_out * lax.rsqrt(
        jnp.mean(recur_out * recur_out, axis=-1, keepdims=True) + norm_eps
    )
    recur_out = recur_out * recur_gain.reshape(count_of_heads, head_k)
    gated = recur_out.reshape(row_count, count_of_heads * head_k) * jax.nn.silu(
        outgate_raw.astype(jnp.float32)
    )
    y_recur = gated.astype(jnp.bfloat16)
    pool_seen, recur_seen = (
        lax.all_to_all(y_pool, "tp", split_axis=0, concat_axis=1, tiled=True),
        lax.all_to_all(y_recur, "tp", split_axis=0, concat_axis=1, tiled=True),
    )
    pieces = sent_together((out_pool, out_recur), "tp", 0, 1)
    running_sum = jnp.dot(pool_seen, pieces[0], preferred_element_type=jnp.float32)
    mixed = running_sum + jnp.dot(recur_seen, pieces[1], preferred_element_type=jnp.float32)
    return mixed.astype(jnp.bfloat16)


def solution(mesh):
    split = Mesh(mesh.devices.reshape(4, 4, 2, mesh.shape["tp"]), ("sp_0", "sp_1", "sp_2", "tp"))
    placed = (
        P(SP, None),
        P(),
        P(None, "tp"),
        P(None, "tp"),
        P(None, "tp"),
        P(None, "tp"),
        P(None, "tp"),
        P("tp", None, None),
        P("tp"),
        P("tp"),
        P(SP, "tp"),
        P("tp"),
        P("tp", None, None),
        P("tp", None),
        P("tp", None),
    )
    return jax.shard_map(
        per_device, mesh=split, in_specs=placed, out_specs=P(SP_TP, None), check_vma=False
    )
```

profile of v0, /device:TPU:1, one launch (start us, length us, event | category | flops | bytes accessed | tf_op | source)
XLA Modules:
  0.0 226.8 jit_solution(6997520110999270708)
XLA Ops:
  9.9 4.2 %fusion = f32[1536]{0:T(1024)S(1)} fusion(bf16[1536,2048]{1,0:T(8,128)(2,1)} %param.15), kind=kLoop, calls=%fused_computation.2 | loop fusion | flops 9435648 | bytes 6297600 | tf_op jit(solution)/shard_map/reduce_sum | solution.py:55
  16.0 4.9 %divide_multiply_fusion = (f32[1536,256]{1,0:T(8,128)}, f32[1536,256]{1,0:T(8,128)S(1)}) fusion(f32[256]{0:T(256)S(1)} %get-tuple-element.30, f32[256]{0:T(256)S(1)} %get-tuple-element.32, f32[256]{0:T(256)S(1)} %get-tuple-element.31, bf16[1536,2048]{1,0:T(8,128)(2,1)S(1)} %fusion.2, bf16[2048,256]{1,0:T(8,128)(2,1)S(1)} %copy-done), kind=kOutput, calls=%fused_computation.64 | convolution fusion | flops 1619263488 | bytes 10488832 | tf_op jit(solution)/shard_map/dot_general | solution.py:159
  29.2 6.1 %divide_multiply_fusion.1 = f32[1536,256]{1,0:T(8,128)} fusion(bf16[1536,2048]{1,0:T(8,128)(2,1)} %copy-done.4, bf16[2048,256]{1,0:T(8,128)(2,1)} %param.18), kind=kOutput, calls=%fused_computation.66 | convolution fusion | flops 1612972032 | bytes 8912896 | tf_op jit(solution)/shard_map/dot_general | solution.py:156
  38.2 5.9 %convolution_convert_fusion.1 = bf16[1536,256]{1,0:T(8,128)(2,1)} fusion(bf16[1536,2048]{1,0:T(8,128)(2,1)} %copy-done.4, bf16[2048,256]{1,0:T(8,128)(2,1)} %param.20), kind=kOutput, calls=%fused_computation.18 | convolution fusion | flops 1611005952 | bytes 8126464 | tf_op jit(solution)/shard_map/dot_general | solution.py:162
  44.2 3.5 %bitcast_multiply_fusion.1 = (bf16[2,24,64,128]{3,1,2,0:T(8,128)(2,1)S(1)}, bf16[2,24,64,128]{3,1,2,0:T(8,128)(2,1)}, bf16[2,24,64,128]{3,1,2,0:T(8,128)(2,1)}) fusion(f32[2,24,64,128]{3,1,2,0:T(8,128)S(1)} %fusion.29, f32[24,64,2,128]{3,2,1,0:T(2,128)S(1)} %copy-done.5, f32[2,24,128]{2,1,0:T(8,128)S(1)} %slice_bitcast_fusion.4, ...), kind=kLoop, calls=%fused_computation.47 | loop fusion | flops 3145728 | bytes 7102464 | tf_op jit(solution)/shard_map/mul | solution.py:125
  61.5 8.0 %pad.77 = f32[2,12,128,128]{3,2,1,0:T(8,128)} pad(f32[2,6,128,128]{3,2,1,0:T(8,128)} %add.294, f32[]{:T(128)} %constant.19.clone.1), padding=0_0_0x1_0_1x0_0_0x0_0_0 | pad | bytes 2359300 | tf_op jit(solution)/shard_map/pad | solution.py:173
  69.7 5.0 %pad.76 = f32[2,12,128,128]{3,2,1,0:T(8,128)} pad(f32[2,6,128,128]{3,2,1,0:T(8,128)S(1)} %pad_maximum_fusion.3, f32[]{:T(128)} %constant.19.clone.1), padding=0_0_0x0_1_1x0_0_0x0_0_0 | pad | bytes 2359300 | tf_op jit(solution)/shard_map/pad | solution.py:173
  76.8 9.2 %pad.157 = f32[2,23,128,128]{3,2,1,0:T(8,128)} pad(f32[2,12,128,128]{3,2,1,0:T(8,128)S(1)} %add.296, f32[]{:T(128)} %constant.19.clone.1), padding=0_0_0x0_0_1x0_0_0x0_0_0 | pad | bytes 4587524
  86.0 9.3 %pad.79 = f32[2,24,128,128]{3,2,1,0:T(8,128)} pad(f32[2,12,128,128]{3,2,1,0:T(8,128)S(1)} %add.296, f32[]{:T(128)} %constant.19.clone.1), padding=0_0_0x1_0_1x0_0_0x0_0_0 | pad | bytes 4718596 | tf_op jit(solution)/shard_map/pad | solution.py:173
  102.1 9.2 %pad.78 = f32[2,24,128,128]{3,2,1,0:T(8,128)} pad(f32[2,12,128,128]{3,2,1,0:T(8,128)S(1)} %pad_maximum_fusion.2, f32[]{:T(128)} %constant.19.clone.1), padding=0_0_0x0_1_1x0_0_0x0_0_0 | pad | bytes 4718596 | tf_op jit(solution)/shard_map/pad | solution.py:173
  111.4 8.2 %all-gather.2 = f32[8,1,128]{2,1,0:T(1,128)S(1)} all-gather(f32[2,1,128]{2,1,0:T(1,128)S(1)} %bitcast.219), channel_id=4, replica_groups=mesh['sp_0'=4,'sp_1'=4,'sp_2'=2,'tp'=4] {'sp_1'}, dimensions={0}, use_global_device_ids=true | all-gather | bytes 5120 | tf_op jit(solution)/shard_map/all_gather | solution.py:34
  119.6 8.9 %all_gather.28 = f32[4,2,128]{2,1,0:T(2,128)S(1)} all-gather(f32[1,2,128]{2,1,0:T(2,128)S(1)} %get-tuple-element.21), channel_id=1, replica_groups=mesh['sp_0'=4,'sp_1'=4,'sp_2'=2,'tp'=4] {'sp_0'}, dimensions={0}, use_global_device_ids=true | all-gather | bytes 5120 | tf_op jit(solution)/shard_map/all_gather | solution.py:34
  128.5 6.0 %all-gather.1 = f32[4,1,128,128]{3,2,1,0:T(8,128)S(1)} all-gather(f32[2,1,128,128]{3,2,1,0:T(8,128)S(1)} %slice-done.1), channel_id=3, replica_groups=mesh['sp_0'=4,'sp_1'=4,'sp_2'=2,'tp'=4] {'sp_2'}, dimensions={0}, use_global_device_ids=true | all-gather | bytes 393216 | tf_op jit(solution)/shard_map/all_gather | solution.py:34
  134.6 9.9 %all_gather.30 = f32[4,2,128,128]{3,2,1,0:T(8,128)S(1)} all-gather(f32[1,2,128,128]{3,2,1,0:T(8,128)S(1)} %bitcast_add_fusion.6), channel_id=1, replica_groups=mesh['sp_0'=4,'sp_1'=4,'sp_2'=2,'tp'=4] {'sp_1'}, dimensions={0}, use_global_device_ids=true | all-gather | bytes 655360 | tf_op jit(solution)/shard_map/all_gather | solution.py:34
  144.7 11.2 %all_gather.31 = f32[4,2,128,128]{3,2,1,0:T(8,128)S(1)} all-gather(f32[1,2,128,128]{3,2,1,0:T(8,128)S(1)} %multiply_add_fusion), channel_id=1, replica_groups=mesh['sp_0'=4,'sp_1'=4,'sp_2'=2,'tp'=4] {'sp_0'}, dimensions={0}, use_global_device_ids=true | all-gather | bytes 655360 | tf_op jit(solution)/shard_map/all_gather | solution.py:34
  159.5 3.5 %slice_add_fusion = f32[2,23,128,128]{3,2,1,0:T(8,128)S(1)} fusion(f32[2,24,128,128]{3,2,1,0:T(8,128)} %pad.79, f32[2,24,128,128]{3,2,1,0:T(8,128)} %pad.78), kind=kLoop, calls=%fused_computation.15 | loop fusion | flops 753664 | bytes 9043968 | tf_op jit(solution)/shard_map/add | solution.py:173
  168.1 5.0 %fusion.23 = bf16[1536,256]{1,0:T(8,128)(2,1)S(1)} fusion(f32[192,8,2,128]{3,2,1,0:T(2,128)S(1)} %bitcast.206, f32[192,8,2,128]{3,2,1,0:T(2,128)S(1)} %bitcast.205, bf16[1536,2048]{1,0:T(8,128)(2,1)} %copy-done.4, bf16[2048,256]{1,0:T(8,128)(2,1)S(1)} %copy-done.27, f32[256]{0:T(256)S(1)} %copy-done.29), kind=kOutput, calls=%fused_computation.38 | convolution fusion | flops 1614544896 | bytes 11273216 | tf_op jit(solution)/shard_map/dot_general | solution.py:165
  174.2 3.9 %all-to-all-start.1 = ((bf16[4,384,256]{1,2,0:T(8,128)(2,1)}), bf16[4,384,256]{1,2,0:T(8,128)(2,1)S(1)}, u32[]{:S(2)}, u32[]{:S(2)}) async-start(bf16[4,384,256]{1,2,0:T(8,128)(2,1)} %copy.60), calls=%async_computation.1 | async-start | bytes 1572864 | tf_op jit(solution)/shard_map/all_to_all | solution.py:201
  178.2 4.8 %fusion.90 = (f32[1536,256]{1,0:T(8,128)S(1)}, bf16[1536,256]{1,0:T(8,128)(2,1)S(1)}) fusion(bf16[1536,2048]{1,0:T(8,128)(2,1)} %copy-done.4, bf16[2048,256]{1,0:T(8,128)(2,1)} %param.17), kind=kOutput, calls=%fused_computation.168 | convolution fusion | flops 1611399168 | bytes 9699328 | tf_op jit(solution)/shard_map/dot_general | solution.py:155
  183.0 5.9 %collective-permute-start = (bf16[16,256]{1,0:T(8,128)(2,1)S(1)}, bf16[16,256]{1,0:T(8,128)(2,1)S(1)}, u32[]{:S(2)}, u32[]{:S(2)}) collective-permute-start(bf16[16,256]{1,0:T(8,128)(2,1)S(1)} %slice.296), channel_id=1, source_target_pairs={{0,4},{4,8},{8,12},{12,16},{16,20},{20,24},{24,28},{28,32},{32,36}... | collective-permute-start | bytes 24584 | tf_op jit(solution)/shard_map/ppermute | solution.py:20
  197.3 4.5 %all-to-all-start = ((bf16[4,384,256]{1,2,0:T(8,128)(2,1)}), bf16[4,384,256]{1,2,0:T(8,128)(2,1)S(1)}, u32[]{:S(2)}, u32[]{:S(2)}) async-start(bf16[4,384,256]{1,2,0:T(8,128)(2,1)} %multiply_convert_fusion), calls=%async_computation | async-start | bytes 1572864 | tf_op jit(solution)/shard_map/all_to_all | solution.py:200
  201.8 5.6 %fusion.3 = f32[384,2048]{1,0:T(8,128)} fusion(bf16[384,1024]{0,1:T(8,128)(2,1)S(1)} %bitcast.207, bf16[1024,4096]{1,0:T(8,128)(2,1)} %all-gather.5.cloned.1.call-done), kind=kOutput, calls=%fused_computation.6 | convolution fusion | flops 1610612736 | bytes 8126464 | tf_op jit(solution)/shard_map/dot_general | solution.py:205
  207.4 6.3 %all-to-all-done = bf16[4,384,256]{1,2,0:T(8,128)(2,1)S(1)} async-done(((bf16[4,384,256]{1,2,0:T(8,128)(2,1)}), bf16[4,384,256]{1,2,0:T(8,128)(2,1)S(1)}, u32[]{:S(2)}, u32[]{:S(2)}) %all-to-all-start) | async-done | bytes 786464 | tf_op jit(solution)/shard_map/all_to_all | solution.py:200
  213.7 6.2 %add_convert_fusion = bf16[384,2048]{1,0:T(8,128)(2,1)} fusion(f32[384,2048]{1,0:T(8,128)} %fusion.3, bf16[384,1024]{0,1:T(8,128)(2,1)S(1)} %bitcast.200, bf16[1024,4096]{1,0:T(8,128)(2,1)} %all-gather.5.cloned.1.call-done), kind=kOutput, calls=%fused_computation.10 | convolution fusion | flops 1612185600 | bytes 9699328 | tf_op jit(solution)/shard_map/dot_general | solution.py:204
  (170 shorter events, 57.4 us)
Async XLA Ops:
  6.5 9.4 %copy-start = (bf16[2048,256]{1,0:T(8,128)(2,1)S(1)}, bf16[2048,256]{1,0:T(8,128)(2,1)}, u32[]{:S(2)}) copy-start(bf16[2048,256]{1,0:T(8,128)(2,1)} %param.19) | copy-start | bytes 3145732
  6.5 195.3 %all-gather.5.cloned.1.call-start = ((), (), s32[]{:S(2)}) async-start(), calls=%async_computation.2 | async-start | bytes 10485760 | tf_op jit(solution)/shard_map/all_gather | solution.py:50
  9.8 4.3 %copy-start.26 = (f32[256]{0:T(256)S(1)}, f32[256]{0:T(256)}, u32[]{:S(2)}) copy-start(f32[256]{0:T(256)} %param.24) | copy-start | bytes 3076
  9.8 4.6 %copy-start.2 = (bf16[1536,2048]{1,0:T(8,128)(2,1)S(1)}, bf16[1536,2048]{1,0:T(8,128)(2,1)}, u32[]{:S(2)}) copy-start(bf16[1536,2048]{1,0:T(8,128)(2,1)} %param.15) | copy-start | bytes 18874372
  9.8 4.6 %copy-start.21 = (f32[2048]{0:T(1024)S(1)}, f32[2048]{0:T(1024)}, u32[]{:S(2)}) copy-start(f32[2048]{0:T(1024)} %param.16) | copy-start | bytes 24580
  16.0 4.9 %copy-start.4 = (bf16[1536,2048]{1,0:T(8,128)(2,1)}, bf16[1536,2048]{1,0:T(8,128)(2,1)S(1)}, u32[]{:S(2)}) copy-start(bf16[1536,2048]{1,0:T(8,128)(2,1)S(1)} %fusion.2) | copy-start | bytes 18874372
  25.3 18.9 %copy-start.17 = (f32[2,5,128]{2,1,0:T(8,128)}, f32[2,5,128]{2,1,0:T(8,128)S(1)}, u32[]{:S(2)}) copy-start(f32[2,5,128]{2,1,0:T(8,128)S(1)} %slice.235) | copy-start | bytes 15364
  38.2 5.9 %copy-start.5 = (f32[24,64,2,128]{3,2,1,0:T(2,128)S(1)}, f32[24,64,2,128]{3,2,1,0:T(2,128)}, u32[]{:S(2)}) copy-start(f32[24,64,2,128]{3,2,1,0:T(2,128)} %reshape_reshape.10) | copy-start | bytes 4718596
  38.2 5.9 %copy-start.6 = (f32[24,64,2,128]{3,2,1,0:T(2,128)S(1)}, f32[24,64,2,128]{3,2,1,0:T(2,128)}, u32[]{:S(2)}) copy-start(f32[24,64,2,128]{3,2,1,0:T(2,128)} %reshape_reshape.9) | copy-start | bytes 4718596
  48.2 5.1 %copy-start.11 = (f32[2,12,128]{2,1,0:T(8,128)}, f32[2,12,128]{2,1,0:T(8,128)S(1)}, u32[]{:S(2)}) copy-start(f32[2,12,128]{2,1,0:T(8,128)S(1)} %pad.85) | copy-start | bytes 36868
  48.3 5.1 %copy-start.13 = (f32[2,12,128]{2,1,0:T(8,128)}, f32[2,12,128]{2,1,0:T(8,128)S(1)}, u32[]{:S(2)}) copy-start(f32[2,12,128]{2,1,0:T(8,128)S(1)} %pad.84) | copy-start | bytes 36868
  61.5 8.0 %copy-start.18 = (f32[2,5,128]{2,1,0:T(8,128)S(1)}, f32[2,5,128]{2,1,0:T(8,128)}, u32[]{:S(2)}) copy-start(f32[2,5,128]{2,1,0:T(8,128)} %copy-done.17) | copy-start | bytes 15364
  86.0 9.3 %copy-start.12 = (f32[2,12,128]{2,1,0:T(8,128)S(1)}, f32[2,12,128]{2,1,0:T(8,128)}, u32[]{:S(2)}) copy-start(f32[2,12,128]{2,1,0:T(8,128)} %copy-done.11) | copy-start | bytes 36868
  86.0 9.3 %copy-start.14 = (f32[2,12,128]{2,1,0:T(8,128)S(1)}, f32[2,12,128]{2,1,0:T(8,128)}, u32[]{:S(2)}) copy-start(f32[2,12,128]{2,1,0:T(8,128)} %copy-done.13) | copy-start | bytes 36868
  86.0 9.3 %copy-start.24 = (f32[2,1,128]{2,1,0:T(1,128)S(1)}, f32[2,1,128]{2,1,0:T(1,128)}, u32[]{:S(2)}) copy-start(f32[2,1,128]{2,1,0:T(1,128)} %slice.319) | copy-start | bytes 3076
  102.1 9.3 %copy-start.16 = (f32[2,24,128]{2,1,0:T(8,128)S(1)}, f32[2,24,128]{2,1,0:T(8,128)}, u32[]{:S(2)}) copy-start(f32[2,24,128]{2,1,0:T(8,128)} %pad.87) | copy-start | bytes 73732
  102.1 26.4 %slice-start.1 = ((f32[2,23,128,128]{3,2,1,0:T(8,128)}), f32[2,1,128,128]{3,2,1,0:T(8,128)S(1)}, s32[]{:S(2)}) async-start(f32[2,23,128,128]{3,2,1,0:T(8,128)} %pad.157), calls=%async_computation.4 | async-start | bytes 262144 | tf_op jit(solution)/shard_map/slice | solution.py:175
  111.3 44.6 %copy-start.15 = (f32[2,128,128]{2,1,0:T(8,128)S(1)}, f32[2,128,128]{2,1,0:T(8,128)}, u32[]{:S(2)}) copy-start(f32[2,128,128]{2,1,0:T(8,128)} %param.27) | copy-start | bytes 393220
  144.5 12.0 %copy-start.8 = (bf16[24,64,2,128]{3,2,1,0:T(2,128)(2,1)S(1)}, bf16[24,64,2,128]{3,2,1,0:T(2,128)(2,1)}, u32[]{:S(2)}) copy-start(bf16[24,64,2,128]{3,2,1,0:T(2,128)(2,1)} %copy-done.7) | copy-start | bytes 2359300
  144.5 12.0 %copy-start.9 = (bf16[2,24,64,128]{3,1,2,0:T(8,128)(2,1)S(1)}, bf16[2,24,64,128]{3,1,2,0:T(8,128)(2,1)}, u32[]{:S(2)}) copy-start(bf16[2,24,64,128]{3,1,2,0:T(8,128)(2,1)} %get-tuple-element.14) | copy-start | bytes 2359300
  174.2 23.1 %all-to-all-start.1 = ((bf16[4,384,256]{1,2,0:T(8,128)(2,1)}), bf16[4,384,256]{1,2,0:T(8,128)(2,1)S(1)}, u32[]{:S(2)}, u32[]{:S(2)}) async-start(bf16[4,384,256]{1,2,0:T(8,128)(2,1)} %copy.60), calls=%async_computation.1 | async-start | bytes 1572864 | tf_op jit(solution)/shard_map/all_to_all | solution.py:201
  183.0 7.9 %collective-permute-start = (bf16[16,256]{1,0:T(8,128)(2,1)S(1)}, bf16[16,256]{1,0:T(8,128)(2,1)S(1)}, u32[]{:S(2)}, u32[]{:S(2)}) collective-permute-start(bf16[16,256]{1,0:T(8,128)(2,1)S(1)} %slice.296), channel_id=1, source_target_pairs={{0,4},{4,8},{8,12},{12,16},{16,20},{20,24},{24,28},{28,32},{32,36}... | collective-permute-start | bytes 24584 | tf_op jit(solution)/shard_map/ppermute | solution.py:20
  197.3 16.4 %all-to-all-start = ((bf16[4,384,256]{1,2,0:T(8,128)(2,1)}), bf16[4,384,256]{1,2,0:T(8,128)(2,1)S(1)}, u32[]{:S(2)}, u32[]{:S(2)}) async-start(bf16[4,384,256]{1,2,0:T(8,128)(2,1)} %multiply_convert_fusion), calls=%async_computation | async-start | bytes 1572864 | tf_op jit(solution)/shard_map/all_to_all | solution.py:200
  213.7 6.2 %copy-start.1 = (bf16[2048,256]{1,0:T(8,128)(2,1)S(1)}, bf16[2048,256]{1,0:T(8,128)(2,1)}, u32[]{:S(2)}) copy-start(bf16[2048,256]{1,0:T(8,128)(2,1)} %param.19) | copy-start | bytes 3145732
  (12 other events, 22.6 us)
Sparse Core Ops, SparseCore 0:
  9.9 86.0 all-gather.4
where the time goes:
time: 228 us; the launch traced here: 227 us
  local copies, waits for them, and re-layouts  67.1 us (29%)
  blocking collectives  47.2 us (21%)
  matrix products  45.5 us (20%)
  other arithmetic  30.2 us (13%)
  starting transfers between devices  14.4 us (6%)
  between operations  14.1 us (6%)
  waiting for transfers between devices  8.28 us (4%)
    all_gather x6, blocking collectives, prefix_by_axis(): pieces = jax.tree.map(lambda part: lax.all_gather(part, axis), subtotal)  47.2 us
    pad x14, local copies, waits for them, and re-layouts, per_device(): running = lax.associative_scan(chain, (decays, contrib), axis=1)  35.7 us
    unnamed x62, local copies, waits for them, and re-layouts  13.2 us
    another operation x3, local copies, waits for them, and re-layouts, to_blocks(): array.reshape(block_count, block_len, count_of_heads, head_k)  7.99 us
    add x8, other arithmetic, per_device(): running = lax.associative_scan(chain, (decays, contrib), axis=1)  7.39 us
    all_to_all x1, waiting for transfers between devices, per_device(): lax.all_to_all(y_pool, 'tp', split_axis=0, concat_axis=1, tiled=True)  6.29 us
    dot_general x1, matrix products, per_device(): jnp.dot(pool_seen, pieces[0], preferred_element_type=jnp.float32)  6.21 us
    dot_general x1, matrix products, per_device(): jnp.dot(normed, query_weight, preferred_element_type=jnp.float32)  6.07 us
  transfers between devices with their start and end apart: 4, of which 2 were waited for; matrix products, arithmetic and copies ran while one was open for 58% of the time, Pallas kernels for 0%

commit v1 on v0

v1 whole, which is shorter than its diff:
```python
import functools

import jax
import jax.numpy as jnp
from jax import lax
from jax.experimental import pallas as pl
from jax.experimental.pallas import tpu as pltpu
from jax.sharding import PartitionSpec as P

MESH = pl.DeviceIdType.MESH
F32 = jnp.float32
BF16 = jnp.bfloat16
EPS = 1e-5

ROWS = 1536
CH = 256
NCH = ROWS // CH
BL = 128
NB = ROWS // BL
C = 256
HK = 128
D = 2048
OUT = 384

NT = (((1,), (1,)), ((), ()))
TN = (((0,), (0,)), ((), ()))
NN = (((1,), (0,)), ((), ()))


def dot(a, b, dims=NN):
    return lax.dot_general(a, b, dims, preferred_element_type=F32)


def half_tanh_sigmoid(v):
    return 0.5 + 0.5 * jnp.tanh(0.5 * v)


def log1p_neg(k):
    s = jnp.full_like(k, 1.0 / 8)
    for n in (7, 6, 5, 4, 3, 2):
        s = s * k + 1.0 / n
    return -(k + (k * k) * s)


def kernel(
    x_hbm, gain_hbm, wp_hbm, wq_hbm, wf_hbm, wv_hbm, wg_hbm, mix_hbm, pscale_hbm, lb_hbm,
    extra_hbm, rgain_hbm, init_hbm, op_hbm, or_hbm,
    out_ref,
    xbuf, nbuf, wfv, wqgp, wout, gain, pscale, lb, rgain, extra, mix, init,
    fbuf, vbuf, ebuf, kbuf, qbuf, winbuf, gbuf, pbuf, sloc, run, lrun, vecs,
    totsend, totrecv, ybuf, zbuf, pst, carr, tril, band,
    ypbuf, ypseen, yrbuf, yrseen, acc,
    lsem, w1s, w1r, w2s, w2r, w3s, w3r, es, er, ys, yr_, zs, zr, ps_, pr_, hs, hr, aps, apr, ars, arr,
):
    x = lax.axis_index("tp")
    sp = lax.axis_index("sp")
    c = lax.rem(sp, 2)
    y = lax.rem(lax.div(sp, 2), 4)
    z = lax.div(sp, 8)

    def dev(spi, tpi):
        return {"sp": spi, "tp": tpi}

    def xpeer(k):
        return dev(sp, lax.rem(x + k, 4))

    def ypeer(k):
        return dev(z * 8 + lax.rem(y + k, 4) * 2 + c, x)

    def zpeer(k):
        return dev(lax.rem(z + k, 4) * 8 + y * 2 + c, x)

    sib = dev(sp + 1 - 2 * c, x)
    nxt = dev(lax.rem(sp + 1, 32), x)
    prv = dev(lax.rem(sp + 31, 32), x)

    count = [0]

    def load(src, dst):
        i = count[0]
        count[0] += 1
        cp = pltpu.make_async_copy(src, dst, lsem.at[i])
        cp.start()
        return cp

    def remote(src, dst, ssem, rsem, to):
        cp = pltpu.make_async_remote_copy(
            src_ref=src, dst_ref=dst, send_sem=ssem, recv_sem=rsem, device_id=to, device_id_type=MESH
        )
        return cp

    def rows(i, n):
        return pl.ds(pl.multiple_of(i * n, n), n)

    bar = pltpu.get_barrier_semaphore()
    for k in (1, 2, 3):
        for peer in (xpeer, ypeer, zpeer):
            pl.semaphore_signal(bar, inc=1, device_id=peer(k), device_id_type=MESH)
    for to in (sib, nxt, prv):
        pl.semaphore_signal(bar, inc=1, device_id=to, device_id_type=MESH)

    l_gain = load(gain_hbm, gain)
    l_x = [load(x_hbm.at[pl.ds(0, CH)], xbuf.at[pl.ds(0, CH)])]
    l_wf = load(wf_hbm, wfv.at[:, pl.ds(0, C)])
    l_wv = load(wv_hbm, wfv.at[:, pl.ds(C, C)])
    l_lb = load(lb_hbm, lb)
    l_extra = load(extra_hbm, extra)
    l_x.append(load(x_hbm.at[pl.ds(CH, CH)], xbuf.at[pl.ds(CH, CH)]))
    l_op = load(op_hbm, wout.at[0, rows(x, 256)])
    l_or = load(or_hbm, wout.at[1, rows(x, 256)])
    for i in range(2, NCH):
        l_x.append(load(x_hbm.at[pl.ds(i * CH, CH)], xbuf.at[pl.ds(i * CH, CH)]))
    l_q = load(wq_hbm, wqgp.at[:, pl.ds(0, C)])
    l_g = load(wg_hbm, wqgp.at[:, pl.ds(C, C)])
    l_p = load(wp_hbm, wqgp.at[:, pl.ds(2 * C, C)])
    l_init = load(init_hbm, init)
    l_rg = load(rgain_hbm, rgain)
    l_ps = load(pscale_hbm, pscale)
    l_mix = load(mix_hbm, mix)

    r_i = lax.broadcasted_iota(jnp.int32, (BL, BL), 0)
    c_i = lax.broadcasted_iota(jnp.int32, (BL, BL), 1)
    tril[...] = (c_i <= r_i).astype(F32)
    w = lax.shift_left(jnp.int32(2), x)
    r_w = lax.broadcasted_iota(jnp.int32, (BL, 2 * BL), 0)
    c_w = lax.broadcasted_iota(jnp.int32, (BL, 2 * BL), 1)
    diff = r_w + BL - c_w
    band[...] = jnp.where((diff >= 0) & (diff < w), 1.0, 0.0).astype(BF16)

    def norm(i):
        r = pl.ds(i * CH, CH)
        v = xbuf[r, :].astype(F32)
        rs = lax.rsqrt(jnp.sum(v * v, axis=-1, keepdims=True) * (1.0 / D) + EPS)
        nbuf[r, :] = (v * rs * gain[...]).astype(BF16)

    def proj_fv(i):
        r = pl.ds(i * CH, CH)
        o = dot(nbuf[r, :], wfv[...])
        fbuf[r, :] = o[:, :C]
        vbuf[r, :] = o[:, C:].astype(BF16)

    def state_block(b):
        r = pl.ds(b * BL, BL)
        f = fbuf[r, :]
        key = (1.0 - lb[...]) / (1.0 + jnp.exp(f))
        lf = log1p_neg(key)
        hi = lf.astype(BF16)
        lo = (lf - hi.astype(F32)).astype(BF16)
        t = tril[...]
        tb = t.astype(BF16)
        ones = jnp.ones((2 * BL, HK), BF16)
        cums = []
        for h in range(2):
            hc = slice(h * HK, (h + 1) * HK)
            te = t * extra[h : h + 1, b * BL : (b + 1) * BL]
            te_hi = te.astype(BF16)
            te_lo = (te - te_hi.astype(F32)).astype(BF16)
            lhs = jnp.concatenate([tb, tb, te_hi, te_lo], axis=1)
            rhs = jnp.concatenate([hi[:, hc], lo[:, hc], ones], axis=0)
            cums.append(dot(lhs, rhs))
        cum = jnp.concatenate(cums, axis=1)
        m = cum[BL // 2 - 1 : BL // 2, :]
        last = cum[BL - 1 : BL, :]
        rel = cum - m
        ebuf[r, :] = jnp.exp(rel)
        kd = key * jnp.exp(-rel)
        kbuf[r, :] = kd.astype(BF16)
        kst = (kd * jnp.exp(last - m)).astype(BF16)
        lpre = lrun[...]
        vecs[b, 0:1, :] = lpre
        vecs[b, 1:2, :] = m
        lrun[...] = lpre + last
        a = jnp.exp(last)
        v = vbuf[r, :]
        for h in range(2):
            hc = slice(h * HK, (h + 1) * HK)
            contrib = dot(v[:, hc], kst[:, hc], TN)
            s = run[h]
            sloc[b, h] = s
            run[h] = s * a[:, hc] + contrib

    def proj_qgp(i):
        r = pl.ds(i * CH, CH)
        o = dot(nbuf[r, :], wqgp[...])
        q = o[:, :C]
        qbuf[r, :] = (q * half_tanh_sigmoid(q) * ebuf[r, :]).astype(BF16)
        g = o[:, C : 2 * C]
        gbuf[r, :] = g * half_tanh_sigmoid(g) * rgain[...]
        pbuf[pl.ds(BL + i * CH, CH), :] = o[:, 2 * C :].astype(BF16)

    def score_block(b):
        r = pl.ds(b * BL, BL)
        causal = tril[...] > 0.5
        for h in range(2):
            hc = slice(h * HK, (h + 1) * HK)
            s = dot(qbuf[r, hc], kbuf[r, hc], NT)
            s = jnp.where(causal, s, 0.0).astype(BF16)
            winbuf[r, hc] = dot(s, vbuf[r, hc])

    def pool_block(b):
        ext = pbuf[pl.ds(pl.multiple_of(b * BL, BL), 2 * BL), :]
        sums = dot(band[...], ext)
        t = sp * ROWS + b * BL + lax.broadcasted_iota(jnp.int32, (BL, 1), 0)
        cnt = jnp.minimum(t + 1, w).astype(F32)
        pooled = (sums / cnt - ext[BL:, :].astype(F32)).astype(BF16)
        return (dot(pooled, mix[0]) * pscale[...]).astype(BF16)

    def out_block(b):
        r = pl.ds(pl.multiple_of(b * BL, BL), BL)
        lpre = vecs[b, 0:1, :]
        m = vecs[b, 1:2, :]
        em = jnp.exp(m)
        elm = jnp.exp(lpre + m)
        parts = []
        for h in range(2):
            hc = slice(h * HK, (h + 1) * HK)
            st = (sloc[b, h] * em[:, hc] + carr[h] * elm[:, hc]).astype(BF16)
            o = winbuf[r, hc] + dot(qbuf[r, hc], st, NT)
            ms = jnp.sum(o * o, axis=-1, keepdims=True) * (1.0 / HK)
            parts.append(o * lax.rsqrt(ms + EPS) * gbuf[r, hc])
        return jnp.concatenate(parts, axis=1).astype(BF16)

    l_gain.wait()
    l_x[0].wait()
    norm(0)
    l_wf.wait()
    l_wv.wait()
    l_lb.wait()
    l_extra.wait()
    run[...] = jnp.zeros_like(run)
    lrun[...] = jnp.zeros_like(lrun)
    pbuf[pl.ds(0, BL - 16), :] = jnp.zeros((BL - 16, C), BF16)

    l_op.wait()
    l_or.wait()
    pl.semaphore_wait(bar, 12)
    pa = x * 256 + y * 32
    pb = x * 256 + 128 + z * 32
    w1 = []
    for k in (2, 1, 3):
        for a, at in enumerate((pa, pb)):
            sl = wout.at[c, pl.ds(pl.multiple_of(at, 32), 32)]
            cp = remote(sl, sl, w1s.at[k - 1, a], w1r.at[k - 1, a], xpeer(k))
            cp.start()
            w1.append(cp)

    for i in range(NCH):
        if i + 1 < NCH:
            l_x[i + 1].wait()
        proj_fv(i)
        if i + 1 < NCH:
            norm(i + 1)
        if i > 0:
            state_block(2 * i - 2)
            state_block(2 * i - 1)
    state_block(NB - 2)
    state_block(NB - 1)

    for h in range(2):
        totsend[h, 0:HK, :] = run[h]
        al = jnp.exp(lrun[:, h * HK : (h + 1) * HK])
        totsend[h, HK : HK + 8, :] = jnp.broadcast_to(al, (8, HK))
    e_cp = remote(totsend, totrecv, es, er, sib)
    e_cp.start()
    l_q.wait()
    l_g.wait()
    l_p.wait()
    l_rg.wait()

    def chain(ea, eS, la, lS):
        return ea * la, la * eS + lS

    order = (5, 0, 1, 2, 3, 4)
    pending = {}
    for n, i in enumerate(order):
        proj_qgp(i)
        if n > 0:
            j = order[n - 1]
            score_block(2 * j)
            score_block(2 * j + 1)
        if n == 0:
            h_cp = remote(
                pbuf.at[pl.ds(BL + ROWS - 16, 16)], pbuf.at[pl.ds(BL - 16, 16)], hs, hr, nxt
            )
            h_cp.start()
            e_cp.wait()
            oS, oa = totsend[c, 0:HK, :], totsend[c, HK : HK + 1, :]
            sS, sa = totrecv[c, 0:HK, :], totrecv[c, HK : HK + 1, :]
            first = c == 0
            ea, eS = jnp.where(first, oa, sa), jnp.where(first, oS, sS)
            la, lS = jnp.where(first, sa, oa), jnp.where(first, sS, oS)
            ta, tS = chain(ea, eS, la, lS)
            ybuf[y, 0:HK, :] = tS
            ybuf[y, HK : HK + 8, :] = jnp.broadcast_to(ta, (8, HK))
            y_cp = []
            for k in (2, 1, 3):
                cp = remote(ybuf.at[y], ybuf.at[y], ys.at[k - 1], yr_.at[k - 1], ypeer(k))
                cp.start()
                y_cp.append(cp)
        if n == 2:
            for cp in y_cp:
                cp.wait()
            ta = jnp.ones((1, HK), F32)
            tS = jnp.zeros((HK, HK), F32)
            ya, yS = ta, tS
            for j in range(4):
                ta, tS = chain(ta, tS, ybuf[j, HK : HK + 1, :], ybuf[j, 0:HK, :])
                ya = jnp.where(y > j, ta, ya)
                yS = jnp.where(y > j, tS, yS)
            zbuf[z, 0:HK, :] = tS
            zbuf[z, HK : HK + 8, :] = jnp.broadcast_to(ta, (8, HK))
            pst[0:HK, :] = yS
            pst[HK : HK + 8, :] = jnp.broadcast_to(ya, (8, HK))
            z_cp = []
            for k in (2, 1, 3):
                cp = remote(zbuf.at[z], zbuf.at[z], zs.at[k - 1], zr.at[k - 1], zpeer(k))
                cp.start()
                z_cp.append(cp)
            for cp in w1:
                cp.wait()
            w2 = []
            for k in (2, 1, 3):
                j = lax.rem(x + 4 - k, 4)
                sl = wout.at[c, pl.ds(pl.multiple_of(j * 256 + y * 32, 32), 32)]
                for q in (2, 1, 3):
                    cp = remote(sl, sl, w2s.at[0, k - 1, q - 1], w2r.at[0, k - 1, q - 1], ypeer(q))
                    cp.start()
                    w2.append(cp)
        if n == 4:
            for cp in z_cp:
                cp.wait()
            ta = jnp.ones((1, HK), F32)
            tS = jnp.zeros((HK, HK), F32)
            za, zS = ta, tS
            for j in range(4):
                ta, tS = chain(ta, tS, zbuf[j, HK : HK + 1, :], zbuf[j, 0:HK, :])
                za = jnp.where(z > j, ta, za)
                zS = jnp.where(z > j, tS, zS)
            l_init.wait()
            pa_, pS_ = chain(za, zS, pst[HK : HK + 1, :], pst[0:HK, :])
            carr[c] = pa_ * jnp.transpose(init[c]) + pS_
            p_cp = remote(carr.at[c], carr.at[c], ps_, pr_, sib)
            p_cp.start()
            for k in (2, 1, 3):
                j = lax.rem(x + 4 - k, 4)
                sl = wout.at[c, pl.ds(pl.multiple_of(j * 256 + 128 + z * 32, 32), 32)]
                for q in (2, 1, 3):
                    cp = remote(sl, sl, w2s.at[1, k - 1, q - 1], w2r.at[1, k - 1, q - 1], zpeer(q))
                    cp.start()
                    w2.append(cp)
    score_block(2 * order[-1])
    score_block(2 * order[-1] + 1)

    l_ps.wait()
    l_mix.wait()
    h_cp.wait()

    @pl.when(sp == 0)
    def _():
        pbuf[pl.ds(BL - 16, 16), :] = jnp.zeros((16, C), BF16)

    ap = []
    for k in (2, 1, 3, 0):
        d = lax.rem(x + k, 4)
        for s in range(3):
            blk = pool_block(d * 3 + s)
            if k == 0:
                ypseen[x, pl.ds(s * BL, BL), :] = blk
            else:
                ypbuf[k - 1, pl.ds(s * BL, BL), :] = blk
        if k:
            cp = remote(ypbuf.at[k - 1], ypseen.at[x], aps.at[k - 1], apr.at[k - 1], xpeer(k))
            cp.start()
            ap.append(cp)

    p_cp.wait()
    for h in range(2):
        pcur = carr[h]
        later = totrecv[h, HK : HK + 1, :] * pcur + totrecv[h, 0:HK, :]
        carr[h] = jnp.where(c == 0, pcur, later)
    ar = []
    for k in (2, 1, 3, 0):
        d = lax.rem(x + k, 4)
        for s in range(3):
            blk = out_block(d * 3 + s)
            if k == 0:
                yrseen[x, pl.ds(s * BL, BL), :] = blk
            else:
                yrbuf[k - 1, pl.ds(s * BL, BL), :] = blk
        if k:
            cp = remote(yrbuf.at[k - 1], yrseen.at[x], ars.at[k - 1], arr.at[k - 1], xpeer(k))
            cp.start()
            ar.append(cp)

    for cp in w2:
        cp.wait()
    w3 = []
    for k in (1, 2, 3):
        j = lax.rem(x + 4 - k, 4)
        sl = wout.at[c, rows(j, 256)]
        cp = remote(sl, sl, w3s.at[k - 1], w3r.at[k - 1], sib)
        cp.start()
        w3.append(cp)
    for cp in w3:
        cp.wait()
    for cp in ap:
        cp.wait()
    yp = jnp.concatenate([ypseen[j] for j in range(4)], axis=1)
    for n in range(4):
        nc = pl.ds(n * 512, 512)
        acc[:, nc] = dot(yp, wout[0, :, nc])
    for cp in ar:
        cp.wait()
    yr = jnp.concatenate([yrseen[j] for j in range(4)], axis=1)
    for n in range(4):
        nc = pl.ds(n * 512, 512)
        out_ref[:, nc] = (acc[:, nc] + dot(yr, wout[1, :, nc])).astype(BF16)


def scratch():
    V = pltpu.VMEM
    S = pltpu.SemaphoreType.DMA
    return [
        V((ROWS, D), BF16), V((ROWS, D), BF16), V((D, 2 * C), BF16), V((D, 3 * C), BF16),
        V((2, 4 * C, D), BF16), V((1, D), F32), V((1, C), F32), V((1, C), F32), V((1, C), F32),
        V((2, ROWS), F32), V((1, C, C), BF16), V((2, HK, HK), F32),
        V((ROWS, C), F32), V((ROWS, C), BF16), V((ROWS, C), F32), V((ROWS, C), BF16),
        V((ROWS, C), BF16), V((ROWS, C), F32), V((ROWS, C), F32), V((BL + ROWS, C), BF16),
        V((NB, 2, HK, HK), F32), V((2, HK, HK), F32), V((1, C), F32), V((NB, 2, C), F32),
        V((2, HK + 8, HK), F32), V((2, HK + 8, HK), F32), V((4, HK + 8, HK), F32), V((4, HK + 8, HK), F32),
        V((HK + 8, HK), F32), V((2, HK, HK), F32), V((BL, BL), F32), V((BL, 2 * BL), BF16),
        V((3, OUT, C), BF16), V((4, OUT, C), BF16), V((3, OUT, C), BF16), V((4, OUT, C), BF16),
        V((OUT, D), F32),
        S((20,)), S((3, 2)), S((3, 2)), S((2, 3, 3)), S((2, 3, 3)), S((3,)), S((3,)),
        S(()), S(()), S((3,)), S((3,)), S((3,)), S((3,)), S(()), S(()), S(()), S(()),
        S((3,)), S((3,)), S((3,)), S((3,)),
    ]


def per_device(
    inputs, norm_gain, pool_weight, query_weight, forget_weight, value_weight, outgate_weight,
    pool_mix, pool_scale, lower_bound, extra_decay, recur_gain, init_state, out_pool, out_recur,
):
    anyspec = pl.BlockSpec(memory_space=pl.ANY)
    return pl.pallas_call(
        kernel,
        out_shape=jax.ShapeDtypeStruct((OUT, D), BF16),
        in_specs=[anyspec] * 15,
        out_specs=pl.BlockSpec(memory_space=pltpu.VMEM),
        scratch_shapes=scratch(),
        compiler_params=pltpu.CompilerParams(
            collective_id=0, has_side_effects=True, vmem_limit_bytes=63 * 1024 * 1024
        ),
    )(
        inputs, norm_gain.reshape(1, D), pool_weight, query_weight, forget_weight, value_weight,
        outgate_weight, pool_mix, pool_scale.reshape(1, C), lower_bound.reshape(1, C),
        extra_decay.T, recur_gain.reshape(1, C), init_state, out_pool, out_recur,
    )


def solution(mesh):
    placed = (
        P("sp", None), P(), P(None, "tp"), P(None, "tp"), P(None, "tp"), P(None, "tp"), P(None, "tp"),
        P("tp", None, None), P("tp"), P("tp"), P("sp", "tp"), P("tp"), P("tp", None, None),
        P("tp", None), P("tp", None),
    )
    return jax.shard_map(
        per_device, mesh=mesh, in_specs=placed, out_specs=P(("sp", "tp"), None), check_vma=False
    )
```

time: 228 us -> 60.2 us (0.26)
  local copies, waits for them, and re-layouts: 67.1 us -> 2.73 us
  Pallas kernels: 0 us -> 57.3 us
  blocking collectives: 47.2 us -> 0 us
  matrix products: 45.5 us -> 0 us
  other arithmetic: 30.2 us -> 0 us
  starting transfers between devices: 14.4 us -> 0 us
  between operations: 14.1 us -> 0.01 us
  waiting for transfers between devices: 8.28 us -> 0 us
    pallas_call x0 -> x1, Pallas kernels: none -> 57.3 us  [per_device(): pl.pallas_call(kernel, out_shape=jax.ShapeDtypeStruct((OUT, D), BF16), in...]
    all_gather x6 -> x0, blocking collectives: 47.2 us -> none  [prefix_by_axis(): pieces = jax.tree.map(lambda part: lax.all_gather(part, axis), subtotal)]
    dot_general x11 -> x0, matrix products: 45.5 us -> none  [the longest x1 6.21 us: per_device(): jnp.dot(pool_seen, pieces[0], preferred_element_type=jnp.float32)]
    pad x14 -> x0, local copies, waits for them, and re-layouts: 35.7 us -> none  [per_device(): running = lax.associative_scan(chain, (decays, contrib), axis=1)]
    add x21 -> x0, other arithmetic: 13.5 us -> none  [the longest x8 7.39 us: per_device(): running = lax.associative_scan(chain, (decays, contrib), axis=1)]
    unnamed x62 -> x1, local copies, waits for them, and re-layouts: 13.2 us -> 2.73 us
    all_to_all x2 -> x0, starting transfers between devices: 8.45 us -> none  [the longest x1 4.51 us: per_device(): lax.all_to_all(y_pool, 'tp', split_axis=0, concat_axis=1, tiled=True)]
    another operation x3 -> x0, local copies, waits for them, and re-layouts: 7.99 us -> none  [to_blocks(): array.reshape(block_count, block_len, count_of_heads, head_k)]
  transfers between devices with their start and end apart: 4 -> 0, of which waited for: 2 -> 0; matrix products, arithmetic and copies ran while one was open for 58% -> 0% of each run, Pallas kernels for 0% -> 0%
where the time goes in v1:
time: 60.2 us; the launch traced here: 60.1 us
  Pallas kernels  57.3 us (95%)
  local copies, waits for them, and re-layouts  2.73 us (5%)
    pallas_call x1, Pallas kernels, per_device(): pl.pallas_call(kernel, out_shape=jax.ShapeDtypeStruct((OUT, D), BF16), in...  57.3 us
    unnamed x1, local copies, waits for them, and re-layouts  2.73 us

profile of v1, /device:TPU:1, one launch (start us, length us, event | category | flops | bytes accessed | tf_op | source)
XLA Modules:
  0.0 60.1 jit_solution(7797082495448560970)
XLA Ops:
  0.0 57.3 %shard_map.145 = bf16[384,2048]{1,0:T(8,128)(2,1)} custom-call(bf16[1536,2048]{1,0:T(8,128)(2,1)} %x_hbm.1, f32[1,2048]{1,0:T(1,128)} %bitcast.6, bf16[2048,256]{1,0:T(8,128)(2,1)} %wp_hbm.1, bf16[2048,256]{1,0:T(8,128)(2,1)} %wq_hbm.1, bf16[2048,256]{1,0:T(8,128)(2,1)} %wf_hbm.1, bf16[2048,256]{1,0:T(8,128)(2,1)} %wv_hbm.1, bf16[2048,256]{1,0:T(8,128)(2,1)} %wg_hbm.1, ...), custom_call_target="tpu_custom_call" | custom-call | tf_op jit(solution)/shard_map/pallas_call | solution.py:445
  57.4 2.7 %copy.17 = bf16[384,2048]{1,0:T(8,128)(2,1)} copy(bf16[384,2048]{1,0:T(8,128)(2,1)} %shard_map.145) | data formatting | bytes 3145728

commit v2 on v1

--- a/solution.py
+++ b/solution.py
@@ -46,7 +46,7 @@
     x_hbm, gain_hbm, wp_hbm, wq_hbm, wf_hbm, wv_hbm, wg_hbm, mix_hbm, pscale_hbm, lb_hbm,
     extra_hbm, rgain_hbm, init_hbm, op_hbm, or_hbm,
     out_ref,
-    xbuf, nbuf, wfv, wqgp, wout, gain, pscale, lb, rgain, extra, mix, init,
+    xbuf, nbuf, wfv, wqg, wp, wst, wout, gain, pscale, lb, rgain, extra, mix, init,
     fbuf, vbuf, ebuf, kbuf, qbuf, winbuf, gbuf, pbuf, sloc, run, lrun, vecs,
     totsend, totrecv, ybuf, zbuf, pst, carr, tril, band,
     ypbuf, ypseen, yrbuf, yrseen, acc,
@@ -87,6 +87,7 @@
         cp = pltpu.make_async_remote_copy(
             src_ref=src, dst_ref=dst, send_sem=ssem, recv_sem=rsem, device_id=to, device_id_type=MESH
         )
+        cp.start()
         return cp
 
     def rows(i, n):
@@ -99,24 +100,27 @@
     for to in (sib, nxt, prv):
         pl.semaphore_signal(bar, inc=1, device_id=to, device_id_type=MESH)
 
+    pa = pl.multiple_of(y * 32, 32)
+    pb = pl.multiple_of(128 + z * 32, 32)
     l_gain = load(gain_hbm, gain)
     l_x = [load(x_hbm.at[pl.ds(0, CH)], xbuf.at[pl.ds(0, CH)])]
     l_wf = load(wf_hbm, wfv.at[:, pl.ds(0, C)])
     l_wv = load(wv_hbm, wfv.at[:, pl.ds(C, C)])
     l_lb = load(lb_hbm, lb)
     l_extra = load(extra_hbm, extra)
-    l_x.append(load(x_hbm.at[pl.ds(CH, CH)], xbuf.at[pl.ds(CH, CH)]))
-    l_op = load(op_hbm, wout.at[0, rows(x, 256)])
-    l_or = load(or_hbm, wout.at[1, rows(x, 256)])
-    for i in range(2, NCH):
+    l_pc = [load(op_hbm.at[pl.ds(pa, 32)], wst.at[0, 0]), load(op_hbm.at[pl.ds(pb, 32)], wst.at[0, 1])]
+    l_pc += [load(or_hbm.at[pl.ds(pa, 32)], wst.at[1, 0]), load(or_hbm.at[pl.ds(pb, 32)], wst.at[1, 1])]
+    for i in range(1, NCH):
         l_x.append(load(x_hbm.at[pl.ds(i * CH, CH)], xbuf.at[pl.ds(i * CH, CH)]))
-    l_q = load(wq_hbm, wqgp.at[:, pl.ds(0, C)])
-    l_g = load(wg_hbm, wqgp.at[:, pl.ds(C, C)])
-    l_p = load(wp_hbm, wqgp.at[:, pl.ds(2 * C, C)])
+    l_p = load(wp_hbm, wp)
+    l_q = load(wq_hbm, wqg.at[:, pl.ds(0, C)])
+    l_g = load(wg_hbm, wqg.at[:, pl.ds(C, C)])
     l_init = load(init_hbm, init)
     l_rg = load(rgain_hbm, rgain)
     l_ps = load(pscale_hbm, pscale)
     l_mix = load(mix_hbm, mix)
+    l_op = load(op_hbm, wout.at[0, rows(x, 256)])
+    l_or = load(or_hbm, wout.at[1, rows(x, 256)])
 
     r_i = lax.broadcasted_iota(jnp.int32, (BL, BL), 0)
     c_i = lax.broadcasted_iota(jnp.int32, (BL, BL), 1)
@@ -179,17 +183,20 @@
             sloc[b, h] = s
             run[h] = s * a[:, hc] + contrib
 
-    def proj_qgp(i):
+    def proj_p(i):
         r = pl.ds(i * CH, CH)
-        o = dot(nbuf[r, :], wqgp[...])
+        pbuf[pl.ds(BL + i * CH, CH), :] = dot(nbuf[r, :], wp[...]).astype(BF16)
+
+    def proj_qg(d):
+        r = rows(d, OUT)
+        o = dot(nbuf[r, :], wqg[...])
         q = o[:, :C]
         qbuf[r, :] = (q * half_tanh_sigmoid(q) * ebuf[r, :]).astype(BF16)
-        g = o[:, C : 2 * C]
+        g = o[:, C:]
         gbuf[r, :] = g * half_tanh_sigmoid(g) * rgain[...]
-        pbuf[pl.ds(BL + i * CH, CH), :] = o[:, 2 * C :].astype(BF16)
 
     def score_block(b):
-        r = pl.ds(b * BL, BL)
+        r = rows(b, BL)
         causal = tril[...] > 0.5
         for h in range(2):
             hc = slice(h * HK, (h + 1) * HK)
@@ -220,30 +227,59 @@
             parts.append(o * lax.rsqrt(ms + EPS) * gbuf[r, hc])
         return jnp.concatenate(parts, axis=1).astype(BF16)
 
+    def chain(ea, eS, la, lS):
+        return ea * la, la * eS + lS
+
+    def put_state(ref, a, S):
+        hi = a.astype(BF16)
+        lo = (a - hi.astype(F32)).astype(BF16)
+        ref[0:HK, :] = S.astype(BF16)
+        ref[HK : HK + 8, :] = jnp.broadcast_to(hi, (8, HK))
+        ref[HK + 8 : HK + 16, :] = jnp.broadcast_to(lo, (8, HK))
+
+    def scan_states(ref, me):
+        ta = jnp.ones((1, HK), F32)
+        tS = jnp.zeros((HK, HK), F32)
+        pa_, pS_ = ta, tS
+        for j in range(4):
+            full = ref[j].astype(F32)
+            ta, tS = chain(ta, tS, full[HK : HK + 1, :] + full[HK + 8 : HK + 9, :], full[0:HK, :])
+            pa_ = jnp.where(me > j, ta, pa_)
+            pS_ = jnp.where(me > j, tS, pS_)
+        return ta, tS, pa_, pS_
+
+    w1, w2, w3 = {}, {}, {}
+
+    def w1_send(k):
+        for a, at in enumerate((pa, pb)):
+            dst = wout.at[c, pl.ds(pl.multiple_of(x * 256 + at, 32), 32)]
+            w1[k, a] = remote(wst.at[c, a], dst, w1s.at[k - 1, a], w1r.at[k - 1, a], xpeer(k))
+
+    def w2_send(k, a):
+        w1[k, a].wait_recv()
+        j = lax.rem(x + 4 - k, 4)
+        sl = wout.at[c, pl.ds(pl.multiple_of(j * 256 + (pb if a else pa), 32), 32)]
+        for q in (2, 1, 3):
+            to = (zpeer if a else ypeer)(q)
+            w2[k, a, q] = remote(sl, sl, w2s.at[a, k - 1, q - 1], w2r.at[a, k - 1, q - 1], to)
+
+    def w3_send(k, a):
+        for q in (1, 2, 3):
+            w2[k, a, q].wait_recv()
+        j = lax.rem(x + 4 - k, 4)
+        sl = wout.at[c, pl.ds(pl.multiple_of(j * 256 + a * 128, 128), 128)]
+        w3[k, a] = remote(sl, sl, w3s.at[a, k - 1], w3r.at[a, k - 1], sib)
+
     l_gain.wait()
     l_x[0].wait()
     norm(0)
+    run[...] = jnp.zeros_like(run)
+    lrun[...] = jnp.zeros_like(lrun)
+    pbuf[pl.ds(0, BL - 16), :] = jnp.zeros((BL - 16, C), BF16)
     l_wf.wait()
     l_wv.wait()
     l_lb.wait()
     l_extra.wait()
-    run[...] = jnp.zeros_like(run)
-    lrun[...] = jnp.zeros_like(lrun)
-    pbuf[pl.ds(0, BL - 16), :] = jnp.zeros((BL - 16, C), BF16)
-
-    l_op.wait()
-    l_or.wait()
-    pl.semaphore_wait(bar, 12)
-    pa = x * 256 + y * 32
-    pb = x * 256 + 128 + z * 32
-    w1 = []
-    for k in (2, 1, 3):
-        for a, at in enumerate((pa, pb)):
-            sl = wout.at[c, pl.ds(pl.multiple_of(at, 32), 32)]
-            cp = remote(sl, sl, w1s.at[k - 1, a], w1r.at[k - 1, a], xpeer(k))
-            cp.start()
-            w1.append(cp)
-
     for i in range(NCH):
         if i + 1 < NCH:
             l_x[i + 1].wait()
@@ -253,104 +289,41 @@
         if i > 0:
             state_block(2 * i - 2)
             state_block(2 * i - 1)
+        if i == 0:
+            for cp in l_pc:
+                cp.wait()
+            pl.semaphore_wait(bar, 12)
+            w1_send(1)
+            w1_send(3)
+            w1_send(2)
+        if i == 4:
+            w2_send(1, 0)
     state_block(NB - 2)
     state_block(NB - 1)
+    w2_send(1, 1)
 
     for h in range(2):
         totsend[h, 0:HK, :] = run[h]
         al = jnp.exp(lrun[:, h * HK : (h + 1) * HK])
         totsend[h, HK : HK + 8, :] = jnp.broadcast_to(al, (8, HK))
     e_cp = remote(totsend, totrecv, es, er, sib)
-    e_cp.start()
-    l_q.wait()
-    l_g.wait()
+
     l_p.wait()
-    l_rg.wait()
-
-    def chain(ea, eS, la, lS):
-        return ea * la, la * eS + lS
-
-    order = (5, 0, 1, 2, 3, 4)
-    pending = {}
-    for n, i in enumerate(order):
-        proj_qgp(i)
-        if n > 0:
-            j = order[n - 1]
-            score_block(2 * j)
-            score_block(2 * j + 1)
-        if n == 0:
-            h_cp = remote(
-                pbuf.at[pl.ds(BL + ROWS - 16, 16)], pbuf.at[pl.ds(BL - 16, 16)], hs, hr, nxt
-            )
-            h_cp.start()
-            e_cp.wait()
-            oS, oa = totsend[c, 0:HK, :], totsend[c, HK : HK + 1, :]
-            sS, sa = totrecv[c, 0:HK, :], totrecv[c, HK : HK + 1, :]
-            first = c == 0
-            ea, eS = jnp.where(first, oa, sa), jnp.where(first, oS, sS)
-            la, lS = jnp.where(first, sa, oa), jnp.where(first, sS, oS)
-            ta, tS = chain(ea, eS, la, lS)
-            ybuf[y, 0:HK, :] = tS
-            ybuf[y, HK : HK + 8, :] = jnp.broadcast_to(ta, (8, HK))
-            y_cp = []
-            for k in (2, 1, 3):
-                cp = remote(ybuf.at[y], ybuf.at[y], ys.at[k - 1], yr_.at[k - 1], ypeer(k))
-                cp.start()
-                y_cp.append(cp)
-        if n == 2:
-            for cp in y_cp:
-                cp.wait()
-            ta = jnp.ones((1, HK), F32)
-            tS = jnp.zeros((HK, HK), F32)
-            ya, yS = ta, tS
-            for j in range(4):
-                ta, tS = chain(ta, tS, ybuf[j, HK : HK + 1, :], ybuf[j, 0:HK, :])
-                ya = jnp.where(y > j, ta, ya)
-                yS = jnp.where(y > j, tS, yS)
-            zbuf[z, 0:HK, :] = tS
-            zbuf[z, HK : HK + 8, :] = jnp.broadcast_to(ta, (8, HK))
-            pst[0:HK, :] = yS
-            pst[HK : HK + 8, :] = jnp.broadcast_to(ya, (8, HK))
-            z_cp = []
-            for k in (2, 1, 3):
-                cp = remote(zbuf.at[z], zbuf.at[z], zs.at[k - 1], zr.at[k - 1], zpeer(k))
-                cp.start()
-                z_cp.append(cp)
-            for cp in w1:
-                cp.wait()
-            w2 = []
-            for k in (2, 1, 3):
-                j = lax.rem(x + 4 - k, 4)
-                sl = wout.at[c, pl.ds(pl.multiple_of(j * 256 + y * 32, 32), 32)]
-                for q in (2, 1, 3):
-                    cp = remote(sl, sl, w2s.at[0, k - 1, q - 1], w2r.at[0, k - 1, q - 1], ypeer(q))
-                    cp.start()
-                    w2.append(cp)
-        if n == 4:
-            for cp in z_cp:
-                cp.wait()
-            ta = jnp.ones((1, HK), F32)
-            tS = jnp.zeros((HK, HK), F32)
-            za, zS = ta, tS
-            for j in range(4):
-                ta, tS = chain(ta, tS, zbuf[j, HK : HK + 1, :], zbuf[j, 0:HK, :])
-                za = jnp.where(z > j, ta, za)
-                zS = jnp.where(z > j, tS, zS)
-            l_init.wait()
-            pa_, pS_ = chain(za, zS, pst[HK : HK + 1, :], pst[0:HK, :])
-            carr[c] = pa_ * jnp.transpose(init[c]) + pS_
-            p_cp = remote(carr.at[c], carr.at[c], ps_, pr_, sib)
-            p_cp.start()
-            for k in (2, 1, 3):
-                j = lax.rem(x + 4 - k, 4)
-                sl = wout.at[c, pl.ds(pl.multiple_of(j * 256 + 128 + z * 32, 32), 32)]
-                for q in (2, 1, 3):
-                    cp = remote(sl, sl, w2s.at[1, k - 1, q - 1], w2r.at[1, k - 1, q - 1], zpeer(q))
-                    cp.start()
-                    w2.append(cp)
-    score_block(2 * order[-1])
-    score_block(2 * order[-1] + 1)
-
+    for i in (5, 0, 1):
+        proj_p(i)
+    h_cp = remote(pbuf.at[pl.ds(BL + ROWS - 16, 16)], pbuf.at[pl.ds(BL - 16, 16)], hs, hr, nxt)
+    e_cp.wait()
+    oS, oa = totsend[c, 0:HK, :], totsend[c, HK : HK + 1, :]
+    sS, sa = totrecv[c, 0:HK, :], totrecv[c, HK : HK + 1, :]
+    first = c == 0
+    ea, eS = jnp.where(first, oa, sa), jnp.where(first, oS, sS)
+    la, lS = jnp.where(first, sa, oa), jnp.where(first, sS, oS)
+    put_state(ybuf.at[y], *chain(ea, eS, la, lS))
+    y_cp = [
+        remote(ybuf.at[y], ybuf.at[y], ys.at[k - 1], yr_.at[k - 1], ypeer(k)) for k in (2, 1, 3)
+    ]
+    for i in (2, 3, 4):
+        proj_p(i)
     l_ps.wait()
     l_mix.wait()
     h_cp.wait()
@@ -369,17 +342,17 @@
             else:
                 ypbuf[k - 1, pl.ds(s * BL, BL), :] = blk
         if k:
-            cp = remote(ypbuf.at[k - 1], ypseen.at[x], aps.at[k - 1], apr.at[k - 1], xpeer(k))
-            cp.start()
-            ap.append(cp)
-
-    p_cp.wait()
-    for h in range(2):
-        pcur = carr[h]
-        later = totrecv[h, HK : HK + 1, :] * pcur + totrecv[h, 0:HK, :]
-        carr[h] = jnp.where(c == 0, pcur, later)
+            ap.append(remote(ypbuf.at[k - 1], ypseen.at[x], aps.at[k - 1], apr.at[k - 1], xpeer(k)))
+
+    def do_qg(k):
+        d = lax.rem(x + k, 4)
+        proj_qg(d)
+        for s in range(3):
+            score_block(d * 3 + s)
+
     ar = []
-    for k in (2, 1, 3, 0):
+
+    def do_out(k):
         d = lax.rem(x + k, 4)
         for s in range(3):
             blk = out_block(d * 3 + s)
@@ -388,21 +361,59 @@
             else:
                 yrbuf[k - 1, pl.ds(s * BL, BL), :] = blk
         if k:
-            cp = remote(yrbuf.at[k - 1], yrseen.at[x], ars.at[k - 1], arr.at[k - 1], xpeer(k))
-            cp.start()
-            ar.append(cp)
-
-    for cp in w2:
+            ar.append(remote(yrbuf.at[k - 1], yrseen.at[x], ars.at[k - 1], arr.at[k - 1], xpeer(k)))
+
+    l_q.wait()
+    l_g.wait()
+    l_rg.wait()
+    for cp in y_cp:
         cp.wait()
-    w3 = []
-    for k in (1, 2, 3):
-        j = lax.rem(x + 4 - k, 4)
-        sl = wout.at[c, rows(j, 256)]
-        cp = remote(sl, sl, w3s.at[k - 1], w3r.at[k - 1], sib)
-        cp.start()
-        w3.append(cp)
-    for cp in w3:
+    ta, tS, ya, yS = scan_states(ybuf, y)
+    put_state(zbuf.at[z], ta, tS)
+    pst[0:HK, :] = yS
+    pst[HK : HK + 8, :] = jnp.broadcast_to(ya, (8, HK))
+    z_cp = [
+        remote(zbuf.at[z], zbuf.at[z], zs.at[k - 1], zr.at[k - 1], zpeer(k)) for k in (2, 1, 3)
+    ]
+    w2_send(3, 0)
+    w2_send(2, 0)
+    do_qg(2)
+    for cp in z_cp:
         cp.wait()
+    ta, tS, za, zS = scan_states(zbuf, z)
+    l_init.wait()
+    fa, fS = chain(za, zS, pst[HK : HK + 1, :], pst[0:HK, :])
+    carr[c] = fa * jnp.transpose(init[c]) + fS
+    p_cp = remote(carr.at[c], carr.at[c], ps_, pr_, sib)
+    w2_send(3, 1)
+    w2_send(2, 1)
+    do_qg(1)
+    p_cp.wait()
+    for h in range(2):
+        pcur = carr[h]
+        later = totrecv[h, HK : HK + 1, :] * pcur + totrecv[h, 0:HK, :]
+        carr[h] = jnp.where(c == 0, pcur, later)
+    do_out(2)
+    do_out(1)
+    w3_send(1, 0)
+    w3_send(1, 1)
+    do_qg(3)
+    do_out(3)
+    do_qg(0)
+    do_out(0)
+
+    w3_send(3, 0)
+    w3_send(2, 0)
+    w3_send(3, 1)
+    w3_send(2, 1)
+    for cp in w3.values():
+        cp.wait()
+    for cp in w1.values():
+        cp.wait_send()
+    for cp in w2.values():
+        cp.wait_send()
+    l_op.wait()
+    l_or.wait()
     for cp in ap:
         cp.wait()
     yp = jnp.concatenate([ypseen[j] for j in range(4)], axis=1)
@@ -421,17 +432,18 @@
     V = pltpu.VMEM
     S = pltpu.SemaphoreType.DMA
     return [
-        V((ROWS, D), BF16), V((ROWS, D), BF16), V((D, 2 * C), BF16), V((D, 3 * C), BF16),
+        V((ROWS, D), BF16), V((ROWS, D), BF16), V((D, 2 * C), BF16), V((D, 2 * C), BF16), V((D, C), BF16),
+        V((2, 2, 32, D), BF16),
         V((2, 4 * C, D), BF16), V((1, D), F32), V((1, C), F32), V((1, C), F32), V((1, C), F32),
         V((2, ROWS), F32), V((1, C, C), BF16), V((2, HK, HK), F32),
         V((ROWS, C), F32), V((ROWS, C), BF16), V((ROWS, C), F32), V((ROWS, C), BF16),
         V((ROWS, C), BF16), V((ROWS, C), F32), V((ROWS, C), F32), V((BL + ROWS, C), BF16),
         V((NB, 2, HK, HK), F32), V((2, HK, HK), F32), V((1, C), F32), V((NB, 2, C), F32),
-        V((2, HK + 8, HK), F32), V((2, HK + 8, HK), F32), V((4, HK + 8, HK), F32), V((4, HK + 8, HK), F32),
+        V((2, HK + 8, HK), F32), V((2, HK + 8, HK), F32), V((4, HK + 16, HK), BF16), V((4, HK + 16, HK), BF16),
         V((HK + 8, HK), F32), V((2, HK, HK), F32), V((BL, BL), F32), V((BL, 2 * BL), BF16),
         V((3, OUT, C), BF16), V((4, OUT, C), BF16), V((3, OUT, C), BF16), V((4, OUT, C), BF16),
         V((OUT, D), F32),
-        S((20,)), S((3, 2)), S((3, 2)), S((2, 3, 3)), S((2, 3, 3)), S((3,)), S((3,)),
+        S((24,)), S((3, 2)), S((3, 2)), S((2, 3, 3)), S((2, 3, 3)), S((2, 3)), S((2, 3)),
         S(()), S(()), S((3,)), S((3,)), S((3,)), S((3,)), S(()), S(()), S(()), S(()),
         S((3,)), S((3,)), S((3,)), S((3,)),
     ]

time: 60.2 us -> 49.8 us (0.83)
  Pallas kernels: 57.3 us -> 46.9 us
    pallas_call x1, Pallas kernels: 57.3 us -> 46.9 us  [per_device(): pl.pallas_call(kernel, out_shape=jax.ShapeDtypeStruct((OUT, D), BF16), in...]
where the time goes in v2:
time: 49.8 us; the launch traced here: 49.6 us
  Pallas kernels  46.9 us (94%)
  local copies, waits for them, and re-layouts  2.73 us (5%)
    pallas_call x1, Pallas kernels, per_device(): pl.pallas_call(kernel, out_shape=jax.ShapeDtypeStruct((OUT, D), BF16), in...  46.9 us
    unnamed x1, local copies, waits for them, and re-layouts  2.73 us

profile of v2, /device:TPU:1, one launch (start us, length us, event | category | flops | bytes accessed | tf_op | source)
XLA Modules:
  0.0 49.6 jit_solution(14567259244119341721)
XLA Ops:
  0.0 46.9 %shard_map.145 = bf16[384,2048]{1,0:T(8,128)(2,1)} custom-call(bf16[1536,2048]{1,0:T(8,128)(2,1)} %x_hbm.1, f32[1,2048]{1,0:T(1,128)} %bitcast.6, bf16[2048,256]{1,0:T(8,128)(2,1)} %wp_hbm.1, bf16[2048,256]{1,0:T(8,128)(2,1)} %wq_hbm.1, bf16[2048,256]{1,0:T(8,128)(2,1)} %wf_hbm.1, bf16[2048,256]{1,0:T(8,128)(2,1)} %wv_hbm.1, bf16[2048,256]{1,0:T(8,128)(2,1)} %wg_hbm.1, ...), custom_call_target="tpu_custom_call" | custom-call | tf_op jit(solution)/shard_map/pallas_call | solution.py:457
  46.9 2.7 %copy.17 = bf16[384,2048]{1,0:T(8,128)(2,1)} copy(bf16[384,2048]{1,0:T(8,128)(2,1)} %shard_map.145) | data formatting | bytes 3145728

commit v3 on v2

v3 whole, which is shorter than its diff:
```python
import jax
import jax.numpy as jnp
from jax import lax
from jax.experimental import pallas as pl
from jax.experimental.pallas import tpu as pltpu
from jax.sharding import PartitionSpec as P

MESH = pl.DeviceIdType.MESH
F32 = jnp.float32
BF16 = jnp.bfloat16
EPS = 1e-5

ROWS = 1536
OUT = 384
BL = 128
NB = ROWS // BL
C = 256
HK = 128
D = 2048
PF = HK + 16

NT = (((1,), (1,)), ((), ()))
TN = (((0,), (0,)), ((), ()))
NN = (((1,), (0,)), ((), ()))

LOG2E = 1.4426950408889634
POLY = (-LOG2E, -0.7213472908955184, -0.48097089760573397, -0.3571200043786398, -0.3431147843908393)


def dot(a, b, dims=NN):
    return lax.dot_general(a, b, dims, preferred_element_type=F32)


def silu(v):
    half = 0.5 * v
    return half + half * jnp.tanh(half)


def twice(a):
    return jnp.concatenate([a, a], axis=1)


def diag2(a, b):
    zero = jnp.zeros((HK, HK), BF16)
    top = jnp.concatenate([a, zero], axis=1)
    return jnp.concatenate([top, jnp.concatenate([zero, b], axis=1)], axis=0)


def kernel(
    x_hbm, gain_hbm, wp_hbm, wq_hbm, wf_hbm, wv_hbm, wg_hbm, mix_hbm, pscale_hbm, lb_hbm,
    extra_hbm, rgain_hbm, init_hbm, op_hbm, or_hbm,
    out_ref,
    xbuf, nbuf, wf, wv, wq, wg, wp, wst, wout, gain, pscale, lb, rgain, extra, mix, init,
    rsbuf, ecum, fbuf, vbuf, ebuf, kdiag, vdiag, qbuf, winbuf, gbuf, pbuf, sloc, run, lrun, vecs,
    totsend, totrecv, ybuf, zbuf, pst, carr, trilb, band,
    ypbuf, ypseen, yrbuf, yrseen, acc, obuf,
    lsem, w1s, w1r, w1fs, w1fr, w2s, w2r, w2fs, w2fr, w3s, w3r,
    es, er, ys, yr_, zs, zr, cs, cr, hs, hr, aps, apr, ars, arr, osem,
):
    x = lax.axis_index("tp")
    sp = lax.axis_index("sp")
    c = lax.rem(sp, 2)
    chip = lax.div(sp, 2)
    y = lax.rem(chip, 4)
    z = lax.div(chip, 4)

    def dev(spi, tpi):
        return {"sp": spi, "tp": tpi}

    def xpeer(k):
        return dev(sp, lax.rem(x + k, 4))

    def ypeer(k):
        return dev(z * 8 + lax.rem(y + k, 4) * 2 + c, x)

    def zpeer(k):
        return dev(lax.rem(z + k, 4) * 8 + y * 2 + c, x)

    sib = dev(sp + 1 - 2 * c, x)
    nxt = dev(lax.rem(sp + 1, 32), x)
    prv = dev(lax.rem(sp + 31, 32), x)

    count = [0]

    def load(src, dst):
        i = count[0]
        count[0] += 1
        cp = pltpu.make_async_copy(src, dst, lsem.at[i])
        cp.start()
        return cp

    def remote(src, dst, ssem, rsem, to, start=True):
        cp = pltpu.make_async_remote_copy(
            src_ref=src, dst_ref=dst, send_sem=ssem, recv_sem=rsem, device_id=to, device_id_type=MESH
        )
        if start:
            cp.start()
        return cp

    def rows(i, n):
        return pl.ds(pl.multiple_of(i * n, n), n)

    pa = pl.multiple_of(y * 32, 32)
    pb = pl.multiple_of(128 + z * 32, 32)
    l_extra = load(extra_hbm, extra)
    l_gain = load(gain_hbm, gain)
    l_x = [load(x_hbm.at[pl.ds(0, OUT)], xbuf.at[pl.ds(0, OUT)])]
    l_wf = load(wf_hbm, wf)
    l_wv = load(wv_hbm, wv)
    l_lb = load(lb_hbm, lb)
    l_x.append(load(x_hbm.at[pl.ds(OUT, OUT)], xbuf.at[pl.ds(OUT, OUT)]))
    l_pc = [load(op_hbm.at[pl.ds(pa, 32)], wst.at[0, 0]), load(op_hbm.at[pl.ds(pb, 32)], wst.at[0, 1])]
    l_pc += [load(or_hbm.at[pl.ds(pa, 32)], wst.at[1, 0]), load(or_hbm.at[pl.ds(pb, 32)], wst.at[1, 1])]
    bar = pltpu.get_barrier_semaphore()
    for k in (1, 2, 3):
        for peer in (xpeer, ypeer, zpeer):
            pl.semaphore_signal(bar, inc=1, device_id=peer(k), device_id_type=MESH)
    for to in (sib, nxt, prv):
        pl.semaphore_signal(bar, inc=1, device_id=to, device_id_type=MESH)

    def extra_sums(b):
        parts = []
        for h in range(2):
            e = extra[h : h + 1, b * BL : (b + 1) * BL] * LOG2E
            hi = e.astype(BF16)
            lo = (e - hi.astype(F32)).astype(BF16)
            t = trilb[...]
            parts.append(jnp.concatenate([t * hi, t * lo], axis=1))
        o = dot(jnp.concatenate(parts, axis=0), jnp.ones((2 * BL, HK), BF16))
        r = pl.ds(b * BL, BL)
        ecum[r, 0:HK] = o[:BL]
        ecum[r, HK:] = o[BL:]

    def norm(j):
        g = gain[...].astype(BF16)
        sums = []
        for s in range(3):
            r = pl.ds(j * OUT + s * BL, BL)
            v = xbuf[r, :]
            nbuf[r, :] = v * g
            sq = v * v
            t = [sq[:, i * 256 : (i + 1) * 256] for i in range(8)]
            while len(t) > 1:
                t = [t[i] + t[i + 1] for i in range(0, len(t), 2)]
            sums.append(t[0])
        ss = dot(jnp.concatenate(sums, axis=0), jnp.ones((256, HK), BF16))
        rsbuf[pl.ds(j * OUT, OUT), :] = lax.rsqrt(ss * (1.0 / D) + EPS)

    def proj_fv(j):
        r = pl.ds(j * OUT, OUT)
        n = nbuf[r, :]
        rs = twice(rsbuf[r, :])
        fbuf[r, :] = dot(n, wf[...]) * (0.5 * rs)
        vbuf[r, :] = (dot(n, wv[...]) * rs).astype(BF16)

    def state_block(b):
        r = pl.ds(b * BL, BL)
        half = 0.5 * (1.0 - lb[...])
        key = half - half * jnp.tanh(fbuf[r, :])
        lf = POLY[4] * key + POLY[3]
        for n in (2, 1, 0):
            lf = lf * key + POLY[n]
        lf = lf * key
        hi = lf.astype(BF16)
        lo = (lf - hi.astype(F32)).astype(BF16)
        t = trilb[...]
        cum = dot(twice(t), jnp.concatenate([hi, lo], axis=0)) + ecum[r, :]
        m = cum[BL // 2 - 1 : BL // 2, :]
        last = cum[BL - 1 : BL, :]
        rel = cum - m
        ebuf[r, :] = jnp.exp2(rel)
        kd = (key * jnp.exp2(-rel)).astype(BF16)
        v = vbuf[r, :]
        for h in range(2):
            hc = slice(h * HK, (h + 1) * HK)
            kdiag[b, hc, hc] = kd[:, hc]
            vdiag[b, hc, hc] = v[:, hc]
        lpre = lrun[...]
        vecs[b, 0:1, :] = lpre
        vecs[b, 1:2, :] = m
        lrun[...] = lpre + last
        a = jnp.exp2(last)
        e2 = jnp.exp2(last - m)
        contrib = dot(v, kd, TN)
        for h in range(2):
            hc = slice(h * HK, (h + 1) * HK)
            s = run[h]
            sloc[b, h] = s
            run[h] = s * a[:, hc] + contrib[hc, hc] * e2[:, hc]

    def proj_p(i):
        r = pl.ds(i * OUT, OUT)
        o = dot(nbuf[r, :], wp[...]) * twice(rsbuf[r, :])
        pbuf[pl.ds(BL + i * OUT, OUT), :] = o.astype(BF16)

    def proj_qg(d):
        r = rows(d, OUT)
        n = nbuf[r, :]
        rs = twice(rsbuf[r, :])
        qbuf[r, :] = (silu(dot(n, wq[...]) * rs) * ebuf[r, :]).astype(BF16)
        gbuf[r, :] = silu(dot(n, wg[...]) * rs) * rgain[...]

    def score_block(b):
        r = rows(b, BL)
        s = dot(qbuf[r, :], kdiag[b], NT)
        s = jnp.where(twice(trilb[...]) > 0, s, 0.0).astype(BF16)
        winbuf[r, :] = dot(s, vdiag[b])

    def pool_rows(d):
        parts = []
        for s in range(3):
            b = d * 3 + s
            ext = pbuf[pl.ds(pl.multiple_of(b * BL, BL), 2 * BL), :]
            sums = dot(band[...], ext)
            t = sp * ROWS + b * BL + lax.broadcasted_iota(jnp.int32, (BL, 1), 0)
            cnt = jnp.minimum(t + 1, w).astype(F32)
            parts.append((sums * (1.0 / cnt) - ext[BL:, :].astype(F32)).astype(BF16))
        return (dot(jnp.concatenate(parts, axis=0), mix[0]) * pscale[...]).astype(BF16)

    def out_block(b):
        r = rows(b, BL)
        lpre = vecs[b, 0:1, :]
        m = vecs[b, 1:2, :]
        em = jnp.exp2(m)
        elm = jnp.exp2(lpre + m)
        st = [
            (sloc[b, h] * em[:, h * HK : (h + 1) * HK] + carr[h] * elm[:, h * HK : (h + 1) * HK]).astype(BF16)
            for h in range(2)
        ]
        o = winbuf[r, :] + dot(qbuf[r, :], diag2(st[0], st[1]), NT)
        g = gbuf[r, :]
        parts = []
        for h in range(2):
            hc = slice(h * HK, (h + 1) * HK)
            oh = o[:, hc]
            ms = jnp.sum(oh * oh, axis=-1, keepdims=True) * (1.0 / HK)
            parts.append(oh * lax.rsqrt(ms + EPS) * g[:, hc])
        return jnp.concatenate(parts, axis=1).astype(BF16)

    def chain(ea, eS, la, lS):
        return ea * la, la * eS + lS

    def put_state(ref, a, S):
        hi = a.astype(BF16)
        lo = (a - hi.astype(F32)).astype(BF16)
        ref[0:HK, :] = S.astype(BF16)
        ref[HK : HK + 8, :] = jnp.broadcast_to(hi, (8, HK))
        ref[HK + 8 : HK + 16, :] = jnp.broadcast_to(lo, (8, HK))

    def scan_states(ref, me):
        ta = jnp.ones((1, HK), F32)
        tS = jnp.zeros((HK, HK), F32)
        ea, eS = ta, tS
        for j in range(4):
            full = ref[j].astype(F32)
            ta, tS = chain(ta, tS, full[HK : HK + 1, :] + full[HK + 8 : HK + 9, :], full[0:HK, :])
            ea = jnp.where(me > j, ta, ea)
            eS = jnp.where(me > j, tS, eS)
        return ta, tS, ea, eS

    w1, w1f, w2, w2f, w3 = {}, {}, {}, {}, {}

    def shard_of(k):
        return lax.rem(x + 4 - k, 4)

    def piece(k, a, at, half=None):
        start = shard_of(k) * 256 + a * 128 + at * 32
        if half is None:
            return wout.at[c, pl.ds(pl.multiple_of(start, 32), 32)]
        return wout.at[c, pl.ds(pl.multiple_of(start + half * 16, 16), 16)]

    def mine(a):
        return z if a else y

    def w1_send():
        for a in (1, 0):
            for k in (1, 3):
                w1[k, a] = remote(
                    wst.at[c, a], piece(0, a, mine(a)), w1s.at[k // 2, a], w1r.at[k // 2, a], xpeer(k)
                )

    def w2_first(k, a):
        for q in (1, 3):
            sl = piece(k, a, mine(a))
            to = (zpeer if a else ypeer)(q)
            w2[k, a, q] = remote(sl, sl, w2s.at[a, k - 1, q // 2], w2r.at[a, k - 1, q // 2], to)

    def w1_poll(k, a):
        w1[k, a].wait_recv()
        h = k // 2
        sl = piece(k, a, mine(a), h)
        w1f[h, a] = remote(sl, sl, w1fs.at[h, a], w1fr.at[h, a], xpeer(k))
        w2_first(k, a)

    def w1_poll2(a):
        for h in range(2):
            w1f[h, a].wait_recv()
        w2_first(2, a)

    def w2_poll(k, a):
        for h, q in enumerate((1, 3)):
            w2[k, a, q].wait_recv()
            sl = piece(k, a, lax.rem(mine(a) + 4 - q, 4), h)
            to = (zpeer if a else ypeer)(q)
            w2f[k, a, h] = remote(sl, sl, w2fs.at[a, k - 1, h], w2fr.at[a, k - 1, h], to)
        for q in (0, 1, 3):
            w3_send(k, a, q)

    def w3_send(k, a, q):
        sl = piece(k, a, lax.rem(mine(a) + q, 4))
        w3[k, a, q] = remote(sl, sl, w3s.at[a, k - 1, q], w3r.at[a, k - 1, q], sib)

    def w3_poll(k, a):
        for h in range(2):
            w2f[k, a, h].wait_recv()
        w3_send(k, a, 2)

    r_i = lax.broadcasted_iota(jnp.int32, (BL, BL), 0)
    c_i = lax.broadcasted_iota(jnp.int32, (BL, BL), 1)
    trilb[...] = jnp.where(c_i <= r_i, 1.0, 0.0).astype(BF16)
    w = lax.shift_left(jnp.int32(2), x)
    r_w = lax.broadcasted_iota(jnp.int32, (BL, 2 * BL), 0)
    c_w = lax.broadcasted_iota(jnp.int32, (BL, 2 * BL), 1)
    diff = r_w + BL - c_w
    band[...] = jnp.where((diff >= 0) & (diff < w), 1.0, 0.0).astype(BF16)
    run[...] = jnp.zeros_like(run)
    lrun[...] = jnp.zeros_like(lrun)
    pbuf[pl.ds(0, BL - 16), :] = jnp.zeros((BL - 16, C), BF16)
    for b in range(NB):
        for h in range(2):
            hc, oc = slice(h * HK, (h + 1) * HK), slice((1 - h) * HK, (2 - h) * HK)
            kdiag[b, hc, oc] = jnp.zeros((HK, HK), BF16)
            vdiag[b, hc, oc] = jnp.zeros((HK, HK), BF16)
    l_extra.wait()
    for b in range(NB):
        extra_sums(b)

    l_gain.wait()
    l_x[0].wait()
    norm(0)
    l_wf.wait()
    l_wv.wait()
    l_lb.wait()
    for i in range(2, 4):
        l_x.append(load(x_hbm.at[pl.ds(i * OUT, OUT)], xbuf.at[pl.ds(i * OUT, OUT)]))
    l_p = load(wp_hbm, wp)
    l_q = load(wq_hbm, wq)
    l_g = load(wg_hbm, wg)
    l_init = load(init_hbm, init)
    l_rg = load(rgain_hbm, rgain)
    l_ps = load(pscale_hbm, pscale)
    l_mix = load(mix_hbm, mix)
    l_op = load(op_hbm, wout.at[0, rows(x, 256)])
    l_or = load(or_hbm, wout.at[1, rows(x, 256)])
    for i in range(4):
        if i < 3:
            l_x[i + 1].wait()
        proj_fv(i)
        if i < 3:
            norm(i + 1)
        if i > 0:
            for s in range(3):
                state_block(3 * i - 3 + s)
        if i == 0:
            for cp in l_pc:
                cp.wait()
            pl.semaphore_wait(bar, 12)
            w1_send()
    for s in range(3):
        state_block(9 + s)

    for h in range(2):
        totsend[h, 0:HK, :] = run[h]
        al = jnp.exp2(lrun[:, h * HK : (h + 1) * HK])
        totsend[h, HK : HK + 8, :] = jnp.broadcast_to(al, (8, HK))
    e_cp = remote(totsend, totrecv, es, er, sib)

    w1_poll(1, 1)
    w1_poll(3, 1)
    l_p.wait()
    proj_p(3)
    proj_p(0)
    h_cp = remote(pbuf.at[pl.ds(BL + ROWS - 16, 16)], pbuf.at[pl.ds(BL - 16, 16)], hs, hr, nxt)
    e_cp.wait()
    oS, oa = totsend[c, 0:HK, :], totsend[c, HK : HK + 1, :]
    sS, sa = totrecv[c, 0:HK, :], totrecv[c, HK : HK + 1, :]
    first = c == 0
    ea, eS = jnp.where(first, oa, sa), jnp.where(first, oS, sS)
    la, lS = jnp.where(first, sa, oa), jnp.where(first, sS, oS)
    put_state(ybuf.at[y], *chain(ea, eS, la, lS))
    y_cp = [
        remote(ybuf.at[y], ybuf.at[y], ys.at[k - 1], yr_.at[k - 1], ypeer(k)) for k in (2, 1, 3)
    ]
    w1_poll(1, 0)
    w1_poll(3, 0)
    proj_p(1)
    proj_p(2)
    l_ps.wait()
    l_mix.wait()
    h_cp.wait()

    @pl.when(sp == 0)
    def _():
        pbuf[pl.ds(BL - 16, 16), :] = jnp.zeros((16, C), BF16)

    ap = []
    for k in (2, 1, 3, 0):
        blk = pool_rows(lax.rem(x + k, 4))
        if k:
            ypbuf[k - 1] = blk
            ap.append(remote(ypbuf.at[k - 1], ypseen.at[x], aps.at[k - 1], apr.at[k - 1], xpeer(k)))
        else:
            ypseen[x] = blk

    def do_proj(k):
        proj_qg(lax.rem(x + k, 4))

    def do_scores(k):
        for s in range(3):
            score_block(lax.rem(x + k, 4) * 3 + s)

    def do_qg(k):
        do_proj(k)
        do_scores(k)

    ar = {}

    def do_out(k):
        d = lax.rem(x + k, 4)
        for s in range(3):
            blk = out_block(d * 3 + s)
            if k == 0:
                yrseen[x, pl.ds(s * BL, BL), :] = blk
            else:
                yrbuf[k - 1, pl.ds(s * BL, BL), :] = blk
        if k:
            ar[k] = remote(yrbuf.at[k - 1], yrseen.at[x], ars.at[k - 1], arr.at[k - 1], xpeer(k))

    l_q.wait()
    l_g.wait()
    l_rg.wait()
    do_proj(1)
    for cp in y_cp:
        cp.wait()
    ta, tS, ya, yS = scan_states(ybuf, y)
    put_state(zbuf.at[z], ta, tS)
    pst[0:HK, :] = yS
    pst[HK : HK + 8, :] = jnp.broadcast_to(ya, (8, HK))
    z_cp = [
        remote(zbuf.at[z], zbuf.at[z], zs.at[k - 1], zr.at[k - 1], zpeer(k)) for k in (2, 1, 3)
    ]
    do_scores(1)
    w1_poll2(1)
    w2_poll(1, 1)
    do_qg(3)
    w2_poll(3, 1)
    w1_poll2(0)
    do_qg(2)
    w2_poll(1, 0)
    for cp in z_cp:
        cp.wait()
    ta, tS, za, zS = scan_states(zbuf, z)
    l_init.wait()
    fa, fS = chain(za, zS, pst[HK : HK + 1, :], pst[0:HK, :])
    carr[c] = fa * jnp.transpose(init[c]) + fS
    c_cp = remote(carr.at[c], carr.at[c], cs, cr, sib)
    do_qg(0)
    w2_poll(3, 0)
    w2_poll(2, 1)
    c_cp.wait()
    for h in range(2):
        cur = carr[h]
        later = totrecv[h, HK : HK + 1, :] * cur + totrecv[h, 0:HK, :]
        carr[h] = jnp.where(c == 0, cur, later)
    do_out(1)
    do_out(3)
    do_out(2)
    w3_poll(1, 1)
    w3_poll(3, 1)
    do_out(0)
    w3_poll(1, 0)
    w3_poll(3, 0)
    w2_poll(2, 0)
    l_op.wait()
    l_or.wait()
    for k in (1, 3):
        for a in range(2):
            for q in range(4):
                w3[k, a, q].wait()
    for cp in ap:
        cp.wait()

    def out_dot(parts, nc):
        left = [(yrseen if mat else ypseen)[shard_of(k)] for mat, k in parts]
        right = [wout[mat, rows(shard_of(k), 256), nc] for mat, k in parts]
        return dot(jnp.concatenate(left, axis=1), jnp.concatenate(right, axis=0))

    for n in range(4):
        nc = pl.ds(n * 512, 512)
        acc[:, nc] = out_dot(((0, 0), (0, 1), (0, 3), (1, 0)), nc)
    w3_poll(2, 1)
    w3_poll(2, 0)
    ar[1].wait()
    ar[3].wait()
    for a in range(2):
        for q in range(4):
            w3[2, a, q].wait()
    for n in range(4):
        nc = pl.ds(n * 512, 512)
        acc[:, nc] += out_dot(((0, 2), (1, 1), (1, 3)), nc)
    ar[2].wait()
    outs = []
    for n in range(4):
        nc = pl.ds(n * 512, 512)
        obuf[n] = (acc[:, nc] + out_dot(((1, 2),), nc)).astype(BF16)
        cp = pltpu.make_async_copy(obuf.at[n], out_ref.at[:, nc], osem.at[n])
        cp.start()
        outs.append(cp)
    for group in (w1, w1f, w2, w2f):
        for cp in group.values():
            cp.wait_send()
    for cp in outs:
        cp.wait()


def scratch():
    V = pltpu.VMEM
    S = pltpu.SemaphoreType.DMA
    return [
        V((ROWS, D), BF16), V((ROWS, D), BF16), V((D, C), BF16), V((D, C), BF16), V((D, C), BF16),
        V((D, C), BF16), V((D, C), BF16),         V((2, 2, 32, D), BF16), V((2, 4 * C, D), BF16),
        V((1, D), F32), V((1, C), F32), V((1, C), F32), V((1, C), F32),
        V((2, ROWS), F32), V((1, C, C), BF16), V((2, HK, HK), F32),
        V((ROWS, HK), F32), V((ROWS, C), F32), V((ROWS, C), F32), V((ROWS, C), BF16), V((ROWS, C), F32),
        V((NB, C, C), BF16), V((NB, C, C), BF16), V((ROWS, C), BF16), V((ROWS, C), F32), V((ROWS, C), F32),
        V((BL + ROWS, C), BF16), V((NB, 2, HK, HK), F32), V((2, HK, HK), F32), V((1, C), F32), V((NB, 2, C), F32),
        V((2, HK + 8, HK), F32), V((2, HK + 8, HK), F32), V((4, PF, HK), BF16), V((4, PF, HK), BF16), V((HK + 8, HK), F32), V((2, HK, HK), F32),
        V((BL, BL), BF16), V((BL, 2 * BL), BF16),
        V((3, OUT, C), BF16), V((4, OUT, C), BF16), V((3, OUT, C), BF16), V((4, OUT, C), BF16),
        V((OUT, D), F32), V((4, OUT, 512), BF16),
        S((24,)), S((2, 2)), S((2, 2)), S((2, 2)), S((2, 2)), S((2, 3, 2)), S((2, 3, 2)), S((2, 3, 2)), S((2, 3, 2)),
        S((2, 3, 4)), S((2, 3, 4)),
        S(()), S(()), S((3,)), S((3,)), S((3,)), S((3,)), S(()), S(()), S(()), S(()), S((3,)), S((3,)), S((3,)), S((3,)),
        S((4,)),
    ]


def per_device(
    inputs, norm_gain, pool_weight, query_weight, forget_weight, value_weight, outgate_weight,
    pool_mix, pool_scale, lower_bound, extra_decay, recur_gain, init_state, out_pool, out_recur,
):
    anyspec = pl.BlockSpec(memory_space=pl.ANY)
    return pl.pallas_call(
        kernel,
        out_shape=jax.ShapeDtypeStruct((OUT, D), BF16),
        in_specs=[anyspec] * 15,
        out_specs=anyspec,
        scratch_shapes=scratch(),
        compiler_params=pltpu.CompilerParams(
            collective_id=0, has_side_effects=True, vmem_limit_bytes=63 * 1024 * 1024
        ),
    )(
        inputs, norm_gain.reshape(1, D), pool_weight, query_weight, forget_weight, value_weight,
        outgate_weight, pool_mix, pool_scale.reshape(1, C), lower_bound.reshape(1, C),
        extra_decay.T, recur_gain.reshape(1, C), init_state, out_pool, out_recur,
    )


def solution(mesh):
    placed = (
        P("sp", None), P(), P(None, "tp"), P(None, "tp"), P(None, "tp"), P(None, "tp"), P(None, "tp"),
        P("tp", None, None), P("tp"), P("tp"), P("sp", "tp"), P("tp"), P("tp", None, None),
        P("tp", None), P("tp", None),
    )
    return jax.shard_map(
        per_device, mesh=mesh, in_specs=placed, out_specs=P(("sp", "tp"), None), check_vma=False
    )
```

time: 49.8 us -> 43.9 us (0.88)
  Pallas kernels: 46.9 us -> 41.1 us
    pallas_call x1, Pallas kernels: 46.9 us -> 41.1 us  [per_device(): pl.pallas_call(kernel, out_shape=jax.ShapeDtypeStruct((OUT, D), BF16), in...]
where the time goes in v3:
time: 43.9 us; the launch traced here: 43.8 us
  Pallas kernels  41.1 us (94%)
  local copies, waits for them, and re-layouts  2.73 us (6%)
    pallas_call x1, Pallas kernels, per_device(): pl.pallas_call(kernel, out_shape=jax.ShapeDtypeStruct((OUT, D), BF16), in...  41.1 us
    unnamed x1, local copies, waits for them, and re-layouts  2.73 us

profile of v3, /device:TPU:1, one launch (start us, length us, event | category | flops | bytes accessed | tf_op | source)
XLA Modules:
  0.0 43.8 jit_solution(6277086601377569836)
XLA Ops:
  0.0 41.1 %shard_map.145 = bf16[384,2048]{1,0:T(8,128)(2,1)} custom-call(bf16[1536,2048]{1,0:T(8,128)(2,1)} %x_hbm.1, f32[1,2048]{1,0:T(1,128)} %bitcast.6, bf16[2048,256]{1,0:T(8,128)(2,1)} %wp_hbm.1, bf16[2048,256]{1,0:T(8,128)(2,1)} %wq_hbm.1, bf16[2048,256]{1,0:T(8,128)(2,1)} %wf_hbm.1, bf16[2048,256]{1,0:T(8,128)(2,1)} %wv_hbm.1, bf16[2048,256]{1,0:T(8,128)(2,1)} %wg_hbm.1, ...), custom_call_target="tpu_custom_call" | custom-call | tf_op jit(solution)/shard_map/pallas_call | solution.py:553
  41.1 2.7 %copy.17 = bf16[384,2048]{1,0:T(8,128)(2,1)} copy(bf16[384,2048]{1,0:T(8,128)(2,1)} %shard_map.145) | data formatting | bytes 3145728

commit v4 on v3

--- a/solution.py
+++ b/solution.py
@@ -115,8 +115,16 @@
     for k in (1, 2, 3):
         for peer in (xpeer, ypeer, zpeer):
             pl.semaphore_signal(bar, inc=1, device_id=peer(k), device_id_type=MESH)
-    for to in (sib, nxt, prv):
-        pl.semaphore_signal(bar, inc=1, device_id=to, device_id_type=MESH)
+    pl.semaphore_signal(bar, inc=1, device_id=sib, device_id_type=MESH)
+
+    @pl.when(sp < 31)
+    def _():
+        pl.semaphore_signal(bar, inc=1, device_id=nxt, device_id_type=MESH)
+
+    @pl.when(sp > 0)
+    def _():
+        pl.semaphore_signal(bar, inc=1, device_id=prv, device_id_type=MESH)
+
 
     def extra_sums(b):
         parts = []
@@ -364,7 +372,7 @@
         if i == 0:
             for cp in l_pc:
                 cp.wait()
-            pl.semaphore_wait(bar, 12)
+            pl.semaphore_wait(bar, jnp.where((sp == 0) | (sp == 31), 11, 12))
             w1_send()
     for s in range(3):
         state_block(9 + s)
@@ -375,12 +383,17 @@
         totsend[h, HK : HK + 8, :] = jnp.broadcast_to(al, (8, HK))
     e_cp = remote(totsend, totrecv, es, er, sib)
 
-    w1_poll(1, 1)
-    w1_poll(3, 1)
     l_p.wait()
     proj_p(3)
     proj_p(0)
-    h_cp = remote(pbuf.at[pl.ds(BL + ROWS - 16, 16)], pbuf.at[pl.ds(BL - 16, 16)], hs, hr, nxt)
+    h_cp = remote(pbuf.at[pl.ds(BL + ROWS - 16, 16)], pbuf.at[pl.ds(BL - 16, 16)], hs, hr, nxt, False)
+
+    @pl.when(sp < 31)
+    def _():
+        h_cp.start()
+
+    w1_poll(1, 1)
+    w1_poll(3, 1)
     e_cp.wait()
     oS, oa = totsend[c, 0:HK, :], totsend[c, HK : HK + 1, :]
     sS, sa = totrecv[c, 0:HK, :], totrecv[c, HK : HK + 1, :]
@@ -397,20 +410,33 @@
     proj_p(2)
     l_ps.wait()
     l_mix.wait()
-    h_cp.wait()
+    @pl.when(sp < 31)
+    def _():
+        h_cp.wait_send()
+
+    @pl.when(sp > 0)
+    def _():
+        h_cp.wait_recv()
 
     @pl.when(sp == 0)
     def _():
         pbuf[pl.ds(BL - 16, 16), :] = jnp.zeros((16, C), BF16)
 
-    ap = []
-    for k in (2, 1, 3, 0):
-        blk = pool_rows(lax.rem(x + k, 4))
-        if k:
-            ypbuf[k - 1] = blk
-            ap.append(remote(ypbuf.at[k - 1], ypseen.at[x], aps.at[k - 1], apr.at[k - 1], xpeer(k)))
-        else:
-            ypseen[x] = blk
+    ap = {}
+
+    def do_pool(ks):
+        blks = [pool_rows(lax.rem(x + k, 4)) for k in ks]
+        for k, blk in zip(ks, blks):
+            if k:
+                ypbuf[k - 1] = blk
+            else:
+                ypseen[x] = blk
+        for k in ks:
+            if k:
+                ap[k] = remote(ypbuf.at[k - 1], ypseen.at[x], aps.at[k - 1], apr.at[k - 1], xpeer(k))
+
+    do_pool((1, 3))
+    do_pool((2, 0))
 
     def do_proj(k):
         proj_qg(lax.rem(x + k, 4))
@@ -425,16 +451,17 @@
 
     ar = {}
 
-    def do_out(k):
-        d = lax.rem(x + k, 4)
-        for s in range(3):
-            blk = out_block(d * 3 + s)
-            if k == 0:
-                yrseen[x, pl.ds(s * BL, BL), :] = blk
-            else:
-                yrbuf[k - 1, pl.ds(s * BL, BL), :] = blk
-        if k:
-            ar[k] = remote(yrbuf.at[k - 1], yrseen.at[x], ars.at[k - 1], arr.at[k - 1], xpeer(k))
+    def do_out(ks):
+        blks = [[out_block(lax.rem(x + k, 4) * 3 + s) for s in range(3)] for k in ks]
+        for k, blk in zip(ks, blks):
+            for s in range(3):
+                if k:
+                    yrbuf[k - 1, pl.ds(s * BL, BL), :] = blk[s]
+                else:
+                    yrseen[x, pl.ds(s * BL, BL), :] = blk[s]
+        for k in ks:
+            if k:
+                ar[k] = remote(yrbuf.at[k - 1], yrseen.at[x], ars.at[k - 1], arr.at[k - 1], xpeer(k))
 
     l_q.wait()
     l_g.wait()
@@ -446,49 +473,44 @@
     put_state(zbuf.at[z], ta, tS)
     pst[0:HK, :] = yS
     pst[HK : HK + 8, :] = jnp.broadcast_to(ya, (8, HK))
-    z_cp = [
-        remote(zbuf.at[z], zbuf.at[z], zs.at[k - 1], zr.at[k - 1], zpeer(k)) for k in (2, 1, 3)
-    ]
+    z_cp = {
+        k: remote(zbuf.at[z], zbuf.at[z], zs.at[k - 1], zr.at[k - 1], zpeer(k), False) for k in (2, 1, 3)
+    }
+    for k, cp in z_cp.items():
+        pl.when(z + k < 4)(cp.start)
     do_scores(1)
+    do_qg(3)
+    w1_poll2(0)
     w1_poll2(1)
-    w2_poll(1, 1)
-    do_qg(3)
-    w2_poll(3, 1)
-    w1_poll2(0)
-    do_qg(2)
-    w2_poll(1, 0)
-    for cp in z_cp:
-        cp.wait()
+    do_proj(2)
+    for k, cp in z_cp.items():
+        pl.when(z >= k)(cp.wait_recv)
     ta, tS, za, zS = scan_states(zbuf, z)
     l_init.wait()
     fa, fS = chain(za, zS, pst[HK : HK + 1, :], pst[0:HK, :])
     carr[c] = fa * jnp.transpose(init[c]) + fS
     c_cp = remote(carr.at[c], carr.at[c], cs, cr, sib)
-    do_qg(0)
-    w2_poll(3, 0)
-    w2_poll(2, 1)
+    do_scores(2)
+    w2_poll(1, 1)
+    w2_poll(1, 0)
+    w2_poll(3, 1)
     c_cp.wait()
     for h in range(2):
         cur = carr[h]
         later = totrecv[h, HK : HK + 1, :] * cur + totrecv[h, 0:HK, :]
         carr[h] = jnp.where(c == 0, cur, later)
-    do_out(1)
-    do_out(3)
-    do_out(2)
+    do_out((1, 3))
+    do_out((2,))
+    w2_poll(3, 0)
+    do_qg(0)
+    w2_poll(2, 1)
+    w2_poll(2, 0)
+    do_out((0,))
     w3_poll(1, 1)
+    w3_poll(1, 0)
     w3_poll(3, 1)
-    do_out(0)
-    w3_poll(1, 0)
-    w3_poll(3, 0)
-    w2_poll(2, 0)
     l_op.wait()
     l_or.wait()
-    for k in (1, 3):
-        for a in range(2):
-            for q in range(4):
-                w3[k, a, q].wait()
-    for cp in ap:
-        cp.wait()
 
     def out_dot(parts, nc):
         left = [(yrseen if mat else ypseen)[shard_of(k)] for mat, k in parts]
@@ -497,17 +519,22 @@
 
     for n in range(4):
         nc = pl.ds(n * 512, 512)
-        acc[:, nc] = out_dot(((0, 0), (0, 1), (0, 3), (1, 0)), nc)
+        acc[:, nc] = out_dot(((0, 0), (1, 0)), nc)
+    w3_poll(3, 0)
     w3_poll(2, 1)
     w3_poll(2, 0)
+    for cp in ap.values():
+        cp.wait()
+    for cp in w3.values():
+        cp.wait()
+    for n in range(4):
+        nc = pl.ds(n * 512, 512)
+        acc[:, nc] += out_dot(((0, 1), (0, 3), (0, 2)), nc)
     ar[1].wait()
     ar[3].wait()
-    for a in range(2):
-        for q in range(4):
-            w3[2, a, q].wait()
     for n in range(4):
         nc = pl.ds(n * 512, 512)
-        acc[:, nc] += out_dot(((0, 2), (1, 1), (1, 3)), nc)
+        acc[:, nc] += out_dot(((1, 1), (1, 3)), nc)
     ar[2].wait()
     outs = []
     for n in range(4):
@@ -516,11 +543,26 @@
         cp = pltpu.make_async_copy(obuf.at[n], out_ref.at[:, nc], osem.at[n])
         cp.start()
         outs.append(cp)
+    for k, cp in z_cp.items():
+        pl.when(z + k < 4)(cp.wait_send)
     for group in (w1, w1f, w2, w2f):
         for cp in group.values():
             cp.wait_send()
     for cp in outs:
         cp.wait()
+
+
+def copy_out(src, dst, buf, sin, sout):
+    n = OUT // 4
+    into = [pltpu.make_async_copy(src.at[pl.ds(i * n, n)], buf.at[i], sin.at[i]) for i in range(4)]
+    out = [pltpu.make_async_copy(buf.at[i], dst.at[pl.ds(i * n, n)], sout.at[i]) for i in range(4)]
+    for cp in into:
+        cp.start()
+    for cp, to in zip(into, out):
+        cp.wait()
+        to.start()
+    for to in out:
+        to.wait()
 
 
 def scratch():
@@ -550,7 +592,7 @@
     pool_mix, pool_scale, lower_bound, extra_decay, recur_gain, init_state, out_pool, out_recur,
 ):
     anyspec = pl.BlockSpec(memory_space=pl.ANY)
-    return pl.pallas_call(
+    full = pl.pallas_call(
         kernel,
         out_shape=jax.ShapeDtypeStruct((OUT, D), BF16),
         in_specs=[anyspec] * 15,
@@ -564,6 +606,15 @@
         outgate_weight, pool_mix, pool_scale.reshape(1, C), lower_bound.reshape(1, C),
         extra_decay.T, recur_gain.reshape(1, C), init_state, out_pool, out_recur,
     )
+    return pl.pallas_call(
+        copy_out,
+        out_shape=jax.ShapeDtypeStruct((OUT, D), BF16),
+        in_specs=[anyspec],
+        out_specs=anyspec,
+        scratch_shapes=[
+            pltpu.VMEM((4, OUT // 4, D), BF16), pltpu.SemaphoreType.DMA((4,)), pltpu.SemaphoreType.DMA((4,)),
+        ],
+    )(full)
 
 
 def solution(mesh):

time: 43.9 us -> 41.3 us (0.941)
  local copies, waits for them, and re-layouts: 2.73 us -> 0 us
    unnamed x1 -> x0, local copies, waits for them, and re-layouts: 2.73 us -> none
    pallas_call x1, Pallas kernels: 41.1 us -> 38.8 us  [per_device(): pl.pallas_call(kernel, out_shape=jax.ShapeDtypeStruct((OUT, D), BF16), in...]
    pallas_call x0 -> x1, Pallas kernels: none -> 2.2 us  [per_device(): pl.pallas_call(copy_out, out_shape=jax.ShapeDtypeStruct((OUT, D), BF16),...]
where the time goes in v4:
time: 41.3 us; the launch traced here: 41.1 us
  Pallas kernels  41 us (99%)
    pallas_call x1, Pallas kernels, per_device(): pl.pallas_call(kernel, out_shape=jax.ShapeDtypeStruct((OUT, D), BF16), in...  38.8 us
    pallas_call x1, Pallas kernels, per_device(): pl.pallas_call(copy_out, out_shape=jax.ShapeDtypeStruct((OUT, D), BF16),...  2.2 us

profile of v4, /device:TPU:1, one launch (start us, length us, event | category | flops | bytes accessed | tf_op | source)
XLA Modules:
  0.0 41.1 jit_solution(4221634846314708894)
XLA Ops:
  0.0 38.8 %shard_map.145.src = bf16[384,2048]{1,0:T(8,128)(2,1)} custom-call(bf16[1536,2048]{1,0:T(8,128)(2,1)} %x_hbm.1, f32[1,2048]{1,0:T(1,128)} %bitcast.6, bf16[2048,256]{1,0:T(8,128)(2,1)} %wp_hbm.1, bf16[2048,256]{1,0:T(8,128)(2,1)} %wq_hbm.1, bf16[2048,256]{1,0:T(8,128)(2,1)} %wf_hbm.1, bf16[2048,256]{1,0:T(8,128)(2,1)} %wv_hbm.1, bf16[2048,256]{1,0:T(8,128)(2,1)} %wg_hbm.1, ...), custom_call_target="tpu_custom_call" | custom-call | tf_op jit(solution)/shard_map/pallas_call | solution.py:595
  38.8 2.2 %shard_map.146 = bf16[384,2048]{1,0:T(8,128)(2,1)} custom-call(bf16[384,2048]{1,0:T(8,128)(2,1)} %shard_map.145.src), custom_call_target="tpu_custom_call" | custom-call | tf_op jit(solution)/shard_map/pallas_call | solution.py:609

commit v5 on v4

--- a/solution.py
+++ b/solution.py
@@ -108,9 +108,6 @@
     l_wf = load(wf_hbm, wf)
     l_wv = load(wv_hbm, wv)
     l_lb = load(lb_hbm, lb)
-    l_x.append(load(x_hbm.at[pl.ds(OUT, OUT)], xbuf.at[pl.ds(OUT, OUT)]))
-    l_pc = [load(op_hbm.at[pl.ds(pa, 32)], wst.at[0, 0]), load(op_hbm.at[pl.ds(pb, 32)], wst.at[0, 1])]
-    l_pc += [load(or_hbm.at[pl.ds(pa, 32)], wst.at[1, 0]), load(or_hbm.at[pl.ds(pb, 32)], wst.at[1, 1])]
     bar = pltpu.get_barrier_semaphore()
     for k in (1, 2, 3):
         for peer in (xpeer, ypeer, zpeer):
@@ -346,10 +343,9 @@
     l_gain.wait()
     l_x[0].wait()
     norm(0)
-    l_wf.wait()
-    l_wv.wait()
-    l_lb.wait()
-    for i in range(2, 4):
+    l_pc = [load(op_hbm.at[pl.ds(pa, 32)], wst.at[0, 0]), load(op_hbm.at[pl.ds(pb, 32)], wst.at[0, 1])]
+    l_pc += [load(or_hbm.at[pl.ds(pa, 32)], wst.at[1, 0]), load(or_hbm.at[pl.ds(pb, 32)], wst.at[1, 1])]
+    for i in range(1, 4):
         l_x.append(load(x_hbm.at[pl.ds(i * OUT, OUT)], xbuf.at[pl.ds(i * OUT, OUT)]))
     l_p = load(wp_hbm, wp)
     l_q = load(wq_hbm, wq)
@@ -360,20 +356,29 @@
     l_mix = load(mix_hbm, mix)
     l_op = load(op_hbm, wout.at[0, rows(x, 256)])
     l_or = load(or_hbm, wout.at[1, rows(x, 256)])
-    for i in range(4):
-        if i < 3:
-            l_x[i + 1].wait()
-        proj_fv(i)
-        if i < 3:
-            norm(i + 1)
-        if i > 0:
-            for s in range(3):
-                state_block(3 * i - 3 + s)
-        if i == 0:
-            for cp in l_pc:
-                cp.wait()
-            pl.semaphore_wait(bar, jnp.where((sp == 0) | (sp == 31), 11, 12))
-            w1_send()
+    l_wf.wait()
+    l_wv.wait()
+    l_lb.wait()
+    proj_fv(0)
+    for cp in l_pc:
+        cp.wait()
+    pl.semaphore_wait(bar, jnp.where((sp == 0) | (sp == 31), 11, 12))
+    w1_send()
+    l_x[1].wait()
+    norm(1)
+    l_x[2].wait()
+    proj_fv(1)
+    norm(2)
+    for s in range(3):
+        state_block(s)
+    l_x[3].wait()
+    proj_fv(2)
+    norm(3)
+    for s in range(3):
+        state_block(3 + s)
+    proj_fv(3)
+    for s in range(3):
+        state_block(6 + s)
     for s in range(3):
         state_block(9 + s)
 
@@ -383,6 +388,8 @@
         totsend[h, HK : HK + 8, :] = jnp.broadcast_to(al, (8, HK))
     e_cp = remote(totsend, totrecv, es, er, sib)
 
+    w1_poll(1, 1)
+    w1_poll(3, 1)
     l_p.wait()
     proj_p(3)
     proj_p(0)
@@ -392,8 +399,6 @@
     def _():
         h_cp.start()
 
-    w1_poll(1, 1)
-    w1_poll(3, 1)
     e_cp.wait()
     oS, oa = totsend[c, 0:HK, :], totsend[c, HK : HK + 1, :]
     sS, sa = totrecv[c, 0:HK, :], totrecv[c, HK : HK + 1, :]
@@ -404,12 +409,12 @@
     y_cp = [
         remote(ybuf.at[y], ybuf.at[y], ys.at[k - 1], yr_.at[k - 1], ypeer(k)) for k in (2, 1, 3)
     ]
-    w1_poll(1, 0)
-    w1_poll(3, 0)
     proj_p(1)
     proj_p(2)
     l_ps.wait()
     l_mix.wait()
+    w1_poll(1, 0)
+    w1_poll(3, 0)
     @pl.when(sp < 31)
     def _():
         h_cp.wait_send()
@@ -478,10 +483,12 @@
     }
     for k, cp in z_cp.items():
         pl.when(z + k < 4)(cp.start)
+    w1_poll2(1)
     do_scores(1)
+    w1_poll2(0)
     do_qg(3)
-    w1_poll2(0)
-    w1_poll2(1)
+    w2_poll(1, 1)
+    w2_poll(3, 1)
     do_proj(2)
     for k, cp in z_cp.items():
         pl.when(z >= k)(cp.wait_recv)
@@ -491,9 +498,8 @@
     carr[c] = fa * jnp.transpose(init[c]) + fS
     c_cp = remote(carr.at[c], carr.at[c], cs, cr, sib)
     do_scores(2)
-    w2_poll(1, 1)
     w2_poll(1, 0)
-    w2_poll(3, 1)
+    w2_poll(3, 0)
     c_cp.wait()
     for h in range(2):
         cur = carr[h]
@@ -501,10 +507,10 @@
         carr[h] = jnp.where(c == 0, cur, later)
     do_out((1, 3))
     do_out((2,))
-    w2_poll(3, 0)
-    do_qg(0)
     w2_poll(2, 1)
+    do_proj(0)
     w2_poll(2, 0)
+    do_scores(0)
     do_out((0,))
     w3_poll(1, 1)
     w3_poll(1, 0)

time: 41.3 us -> 40.3 us (0.976)
  Pallas kernels: 41 us -> 39.8 us
    pallas_call x1, Pallas kernels: 38.8 us -> 37.6 us  [per_device(): pl.pallas_call(kernel, out_shape=jax.ShapeDtypeStruct((OUT, D), BF16), in...]
where the time goes in v5:
time: 40.3 us; the launch traced here: 40 us
  Pallas kernels  39.8 us (99%)
    pallas_call x1, Pallas kernels, per_device(): pl.pallas_call(kernel, out_shape=jax.ShapeDtypeStruct((OUT, D), BF16), in...  37.6 us
    pallas_call x1, Pallas kernels, per_device(): pl.pallas_call(copy_out, out_shape=jax.ShapeDtypeStruct((OUT, D), BF16),...  2.2 us

profile of v5, /device:TPU:1, one launch (start us, length us, event | category | flops | bytes accessed | tf_op | source)
XLA Modules:
  0.0 40.0 jit_solution(17332998511292181016)
XLA Ops:
  0.0 37.6 %shard_map.145.src = bf16[384,2048]{1,0:T(8,128)(2,1)} custom-call(bf16[1536,2048]{1,0:T(8,128)(2,1)} %x_hbm.1, f32[1,2048]{1,0:T(1,128)} %bitcast.6, bf16[2048,256]{1,0:T(8,128)(2,1)} %wp_hbm.1, bf16[2048,256]{1,0:T(8,128)(2,1)} %wq_hbm.1, bf16[2048,256]{1,0:T(8,128)(2,1)} %wf_hbm.1, bf16[2048,256]{1,0:T(8,128)(2,1)} %wv_hbm.1, bf16[2048,256]{1,0:T(8,128)(2,1)} %wg_hbm.1, ...), custom_call_target="tpu_custom_call" | custom-call | tf_op jit(solution)/shard_map/pallas_call | solution.py:601
  37.6 2.2 %shard_map.146 = bf16[384,2048]{1,0:T(8,128)(2,1)} custom-call(bf16[384,2048]{1,0:T(8,128)(2,1)} %shard_map.145.src), custom_call_target="tpu_custom_call" | custom-call | tf_op jit(solution)/shard_map/pallas_call | solution.py:615

commit v6 on v5

--- a/solution.py
+++ b/solution.py
@@ -50,11 +50,11 @@
     x_hbm, gain_hbm, wp_hbm, wq_hbm, wf_hbm, wv_hbm, wg_hbm, mix_hbm, pscale_hbm, lb_hbm,
     extra_hbm, rgain_hbm, init_hbm, op_hbm, or_hbm,
     out_ref,
-    xbuf, nbuf, wf, wv, wq, wg, wp, wst, wout, gain, pscale, lb, rgain, extra, mix, init,
+    xbuf, xhalo, nbuf, wf, wv, wq, wg, wp, wst, wout, gain, pscale, lb, rgain, extra, mix, init,
     rsbuf, ecum, fbuf, vbuf, ebuf, kdiag, vdiag, qbuf, winbuf, gbuf, pbuf, sloc, run, lrun, vecs,
     totsend, totrecv, ybuf, zbuf, pst, carr, trilb, band,
     ypbuf, ypseen, yrbuf, yrseen, acc, obuf,
-    lsem, w1s, w1r, w1fs, w1fr, w2s, w2r, w2fs, w2fr, w3s, w3r,
+    lsem, wsem, w1r, w1fr, w2r, w2fr, w3r,
     es, er, ys, yr_, zs, zr, cs, cr, hs, hr, aps, apr, ars, arr, osem,
 ):
     x = lax.axis_index("tp")
@@ -82,12 +82,15 @@
 
     count = [0]
 
-    def load(src, dst):
-        i = count[0]
-        count[0] += 1
+    def load(src, dst, same=None):
+        i = count[0] if same is None else same
+        count[0] = max(count[0], i + 1)
         cp = pltpu.make_async_copy(src, dst, lsem.at[i])
         cp.start()
         return cp
+
+    def wait_bytes(ref, sem):
+        pltpu.make_async_copy(ref, ref, sem).wait()
 
     def remote(src, dst, ssem, rsem, to, start=True):
         cp = pltpu.make_async_remote_copy(
@@ -105,8 +108,9 @@
     l_extra = load(extra_hbm, extra)
     l_gain = load(gain_hbm, gain)
     l_x = [load(x_hbm.at[pl.ds(0, OUT)], xbuf.at[pl.ds(0, OUT)])]
-    l_wf = load(wf_hbm, wf)
-    l_wv = load(wv_hbm, wv)
+    load(wf_hbm, wf)
+    i_wfv = count[0] - 1
+    load(wv_hbm, wv, i_wfv)
     l_lb = load(lb_hbm, lb)
     bar = pltpu.get_barrier_semaphore()
     for k in (1, 2, 3):
@@ -198,6 +202,17 @@
         o = dot(nbuf[r, :], wp[...]) * twice(rsbuf[r, :])
         pbuf[pl.ds(BL + i * OUT, OUT), :] = o.astype(BF16)
 
+    def proj_first():
+        v = xhalo[...]
+        sq = v * v
+        t = [sq[:, i * 256 : (i + 1) * 256] for i in range(8)]
+        while len(t) > 1:
+            t = [t[i] + t[i + 1] for i in range(0, len(t), 2)]
+        ss = dot(t[0], jnp.ones((256, HK), BF16))
+        rs = jnp.concatenate([lax.rsqrt(ss * (1.0 / D) + EPS), rsbuf[pl.ds(0, OUT), :]], axis=0)
+        n = jnp.concatenate([v * gain[...].astype(BF16), nbuf[pl.ds(0, OUT), :]], axis=0)
+        pbuf[pl.ds(BL - 16, OUT + 16), :] = (dot(n, wp[...]) * twice(rs)).astype(BF16)
+
     def proj_qg(d):
         r = rows(d, OUT)
         n = nbuf[r, :]
@@ -263,7 +278,6 @@
             eS = jnp.where(me > j, tS, eS)
         return ta, tS, ea, eS
 
-    w1, w1f, w2, w2f, w3 = {}, {}, {}, {}, {}
 
     def shard_of(k):
         return lax.rem(x + 4 - k, 4)
@@ -280,44 +294,38 @@
     def w1_send():
         for a in (1, 0):
             for k in (1, 3):
-                w1[k, a] = remote(
-                    wst.at[c, a], piece(0, a, mine(a)), w1s.at[k // 2, a], w1r.at[k // 2, a], xpeer(k)
-                )
+                remote(wst.at[c, a], piece(0, a, mine(a)), wsem, w1r.at[a], xpeer(k))
 
     def w2_first(k, a):
         for q in (1, 3):
             sl = piece(k, a, mine(a))
-            to = (zpeer if a else ypeer)(q)
-            w2[k, a, q] = remote(sl, sl, w2s.at[a, k - 1, q // 2], w2r.at[a, k - 1, q // 2], to)
-
-    def w1_poll(k, a):
-        w1[k, a].wait_recv()
-        h = k // 2
-        sl = piece(k, a, mine(a), h)
-        w1f[h, a] = remote(sl, sl, w1fs.at[h, a], w1fr.at[h, a], xpeer(k))
-        w2_first(k, a)
+            remote(sl, sl, wsem, w2r.at[a, k - 1], (zpeer if a else ypeer)(q))
+
+    def w1_poll(a):
+        wait_bytes(nbuf.at[pl.ds(0, 64)], w1r.at[a])
+        for h, k in enumerate((1, 3)):
+            sl = piece(k, a, mine(a), h)
+            remote(sl, sl, wsem, w1fr.at[a], xpeer(k))
+            w2_first(k, a)
 
     def w1_poll2(a):
-        for h in range(2):
-            w1f[h, a].wait_recv()
+        wait_bytes(nbuf.at[pl.ds(0, 32)], w1fr.at[a])
         w2_first(2, a)
 
+    def w3_send(k, a, q):
+        sl = piece(k, a, lax.rem(mine(a) + q, 4))
+        remote(sl, sl, wsem, w3r, sib)
+
     def w2_poll(k, a):
+        wait_bytes(nbuf.at[pl.ds(0, 64)], w2r.at[a, k - 1])
         for h, q in enumerate((1, 3)):
-            w2[k, a, q].wait_recv()
             sl = piece(k, a, lax.rem(mine(a) + 4 - q, 4), h)
-            to = (zpeer if a else ypeer)(q)
-            w2f[k, a, h] = remote(sl, sl, w2fs.at[a, k - 1, h], w2fr.at[a, k - 1, h], to)
+            remote(sl, sl, wsem, w2fr.at[a, k - 1], (zpeer if a else ypeer)(q))
         for q in (0, 1, 3):
             w3_send(k, a, q)
 
-    def w3_send(k, a, q):
-        sl = piece(k, a, lax.rem(mine(a) + q, 4))
-        w3[k, a, q] = remote(sl, sl, w3s.at[a, k - 1, q], w3r.at[a, k - 1, q], sib)
-
     def w3_poll(k, a):
-        for h in range(2):
-            w2f[k, a, h].wait_recv()
+        wait_bytes(nbuf.at[pl.ds(0, 32)], w2fr.at[a, k - 1])
         w3_send(k, a, 2)
 
     r_i = lax.broadcasted_iota(jnp.int32, (BL, BL), 0)
@@ -343,27 +351,36 @@
     l_gain.wait()
     l_x[0].wait()
     norm(0)
-    l_pc = [load(op_hbm.at[pl.ds(pa, 32)], wst.at[0, 0]), load(op_hbm.at[pl.ds(pb, 32)], wst.at[0, 1])]
-    l_pc += [load(or_hbm.at[pl.ds(pa, 32)], wst.at[1, 0]), load(or_hbm.at[pl.ds(pb, 32)], wst.at[1, 1])]
+    i_pc = count[0]
+    load(op_hbm.at[pl.ds(pa, 32)], wst.at[0, 0], i_pc)
+    load(op_hbm.at[pl.ds(pb, 32)], wst.at[0, 1], i_pc)
+    load(or_hbm.at[pl.ds(pa, 32)], wst.at[1, 0], i_pc)
+    load(or_hbm.at[pl.ds(pb, 32)], wst.at[1, 1], i_pc)
     for i in range(1, 4):
         l_x.append(load(x_hbm.at[pl.ds(i * OUT, OUT)], xbuf.at[pl.ds(i * OUT, OUT)]))
     l_p = load(wp_hbm, wp)
-    l_q = load(wq_hbm, wq)
-    l_g = load(wg_hbm, wg)
+    i_qg = count[0]
+    load(wq_hbm, wq, i_qg)
+    load(wg_hbm, wg, i_qg)
     l_init = load(init_hbm, init)
     l_rg = load(rgain_hbm, rgain)
     l_ps = load(pscale_hbm, pscale)
     l_mix = load(mix_hbm, mix)
-    l_op = load(op_hbm, wout.at[0, rows(x, 256)])
-    l_or = load(or_hbm, wout.at[1, rows(x, 256)])
-    l_wf.wait()
-    l_wv.wait()
+    i_own = count[0]
+    load(op_hbm, wout.at[0, rows(x, 256)], i_own)
+    load(or_hbm, wout.at[1, rows(x, 256)], i_own)
+    wait_bytes(nbuf.at[pl.ds(0, 512)], lsem.at[i_wfv])
     l_lb.wait()
     proj_fv(0)
-    for cp in l_pc:
-        cp.wait()
+    wait_bytes(wst, lsem.at[i_pc])
     pl.semaphore_wait(bar, jnp.where((sp == 0) | (sp == 31), 11, 12))
     w1_send()
+    h_cp = remote(x_hbm.at[pl.ds(ROWS - 16, 16)], xhalo, hs, hr, nxt, False)
+
+    @pl.when(sp < 31)
+    def _():
+        h_cp.start()
+
     l_x[1].wait()
     norm(1)
     l_x[2].wait()
@@ -388,17 +405,10 @@
         totsend[h, HK : HK + 8, :] = jnp.broadcast_to(al, (8, HK))
     e_cp = remote(totsend, totrecv, es, er, sib)
 
-    w1_poll(1, 1)
-    w1_poll(3, 1)
     l_p.wait()
     proj_p(3)
-    proj_p(0)
-    h_cp = remote(pbuf.at[pl.ds(BL + ROWS - 16, 16)], pbuf.at[pl.ds(BL - 16, 16)], hs, hr, nxt, False)
-
-    @pl.when(sp < 31)
-    def _():
-        h_cp.start()
-
+    proj_p(2)
+    w1_poll(1)
     e_cp.wait()
     oS, oa = totsend[c, 0:HK, :], totsend[c, HK : HK + 1, :]
     sS, sa = totrecv[c, 0:HK, :], totrecv[c, HK : HK + 1, :]
@@ -406,15 +416,9 @@
     ea, eS = jnp.where(first, oa, sa), jnp.where(first, oS, sS)
     la, lS = jnp.where(first, sa, oa), jnp.where(first, sS, oS)
     put_state(ybuf.at[y], *chain(ea, eS, la, lS))
-    y_cp = [
-        remote(ybuf.at[y], ybuf.at[y], ys.at[k - 1], yr_.at[k - 1], ypeer(k)) for k in (2, 1, 3)
-    ]
-    proj_p(1)
-    proj_p(2)
-    l_ps.wait()
-    l_mix.wait()
-    w1_poll(1, 0)
-    w1_poll(3, 0)
+    for k in (2, 1, 3):
+        remote(ybuf.at[y], ybuf.at[y], ys, yr_, ypeer(k))
+
     @pl.when(sp < 31)
     def _():
         h_cp.wait_send()
@@ -423,11 +427,16 @@
     def _():
         h_cp.wait_recv()
 
+    proj_p(1)
+    proj_first()
+
     @pl.when(sp == 0)
     def _():
         pbuf[pl.ds(BL - 16, 16), :] = jnp.zeros((16, C), BF16)
 
-    ap = {}
+    l_ps.wait()
+    l_mix.wait()
+    w1_poll(0)
 
     def do_pool(ks):
         blks = [pool_rows(lax.rem(x + k, 4)) for k in ks]
@@ -438,7 +447,7 @@
                 ypseen[x] = blk
         for k in ks:
             if k:
-                ap[k] = remote(ypbuf.at[k - 1], ypseen.at[x], aps.at[k - 1], apr.at[k - 1], xpeer(k))
+                remote(ypbuf.at[k - 1], ypseen.at[x], aps, apr, xpeer(k))
 
     do_pool((1, 3))
     do_pool((2, 0))
@@ -454,7 +463,6 @@
         do_proj(k)
         do_scores(k)
 
-    ar = {}
 
     def do_out(ks):
         blks = [[out_block(lax.rem(x + k, 4) * 3 + s) for s in range(3)] for k in ks]
@@ -466,14 +474,13 @@
                     yrseen[x, pl.ds(s * BL, BL), :] = blk[s]
         for k in ks:
             if k:
-                ar[k] = remote(yrbuf.at[k - 1], yrseen.at[x], ars.at[k - 1], arr.at[k - 1], xpeer(k))
-
-    l_q.wait()
-    l_g.wait()
+                remote(yrbuf.at[k - 1], yrseen.at[x], ars, arr.at[k % 2], xpeer(k))
+
+    wait_bytes(nbuf.at[pl.ds(0, 512)], lsem.at[i_qg])
     l_rg.wait()
     do_proj(1)
-    for cp in y_cp:
-        cp.wait()
+    wait_bytes(ybuf.at[pl.ds(0, 3)], yr_)
+    wait_bytes(ybuf.at[pl.ds(0, 3)], ys)
     ta, tS, ya, yS = scan_states(ybuf, y)
     put_state(zbuf.at[z], ta, tS)
     pst[0:HK, :] = yS
@@ -487,8 +494,6 @@
     do_scores(1)
     w1_poll2(0)
     do_qg(3)
-    w2_poll(1, 1)
-    w2_poll(3, 1)
     do_proj(2)
     for k, cp in z_cp.items():
         pl.when(z >= k)(cp.wait_recv)
@@ -498,8 +503,8 @@
     carr[c] = fa * jnp.transpose(init[c]) + fS
     c_cp = remote(carr.at[c], carr.at[c], cs, cr, sib)
     do_scores(2)
+    w2_poll(1, 1)
     w2_poll(1, 0)
-    w2_poll(3, 0)
     c_cp.wait()
     for h in range(2):
         cur = carr[h]
@@ -507,6 +512,8 @@
         carr[h] = jnp.where(c == 0, cur, later)
     do_out((1, 3))
     do_out((2,))
+    w2_poll(3, 1)
+    w2_poll(3, 0)
     w2_poll(2, 1)
     do_proj(0)
     w2_poll(2, 0)
@@ -515,8 +522,7 @@
     w3_poll(1, 1)
     w3_poll(1, 0)
     w3_poll(3, 1)
-    l_op.wait()
-    l_or.wait()
+    wait_bytes(nbuf.at[pl.ds(0, 512)], lsem.at[i_own])
 
     def out_dot(parts, nc):
         left = [(yrseen if mat else ypseen)[shard_of(k)] for mat, k in parts]
@@ -529,33 +535,26 @@
     w3_poll(3, 0)
     w3_poll(2, 1)
     w3_poll(2, 0)
-    for cp in ap.values():
-        cp.wait()
-    for cp in w3.values():
-        cp.wait()
+    wait_bytes(ypbuf, apr)
+    wait_bytes(ypbuf, aps)
+    wait_bytes(nbuf.at[pl.ds(0, 768)], w3r)
     for n in range(4):
         nc = pl.ds(n * 512, 512)
         acc[:, nc] += out_dot(((0, 1), (0, 3), (0, 2)), nc)
-    ar[1].wait()
-    ar[3].wait()
+    wait_bytes(yrbuf.at[pl.ds(0, 2)], arr.at[1])
     for n in range(4):
         nc = pl.ds(n * 512, 512)
         acc[:, nc] += out_dot(((1, 1), (1, 3)), nc)
-    ar[2].wait()
-    outs = []
+    wait_bytes(yrbuf.at[0], arr.at[0])
     for n in range(4):
         nc = pl.ds(n * 512, 512)
         obuf[n] = (acc[:, nc] + out_dot(((1, 2),), nc)).astype(BF16)
-        cp = pltpu.make_async_copy(obuf.at[n], out_ref.at[:, nc], osem.at[n])
-        cp.start()
-        outs.append(cp)
+        pltpu.make_async_copy(obuf.at[n], out_ref.at[:, nc], osem).start()
     for k, cp in z_cp.items():
         pl.when(z + k < 4)(cp.wait_send)
-    for group in (w1, w1f, w2, w2f):
-        for cp in group.values():
-            cp.wait_send()
-    for cp in outs:
-        cp.wait()
+    wait_bytes(nbuf, wsem)
+    wait_bytes(yrbuf, ars)
+    wait_bytes(nbuf.at[pl.ds(0, OUT)], osem)
 
 
 def copy_out(src, dst, buf, sin, sout):
@@ -575,7 +574,7 @@
     V = pltpu.VMEM
     S = pltpu.SemaphoreType.DMA
     return [
-        V((ROWS, D), BF16), V((ROWS, D), BF16), V((D, C), BF16), V((D, C), BF16), V((D, C), BF16),
+        V((ROWS, D), BF16), V((16, D), BF16), V((ROWS, D), BF16), V((D, C), BF16), V((D, C), BF16), V((D, C), BF16),
         V((D, C), BF16), V((D, C), BF16),         V((2, 2, 32, D), BF16), V((2, 4 * C, D), BF16),
         V((1, D), F32), V((1, C), F32), V((1, C), F32), V((1, C), F32),
         V((2, ROWS), F32), V((1, C, C), BF16), V((2, HK, HK), F32),
@@ -586,10 +585,8 @@
         V((BL, BL), BF16), V((BL, 2 * BL), BF16),
         V((3, OUT, C), BF16), V((4, OUT, C), BF16), V((3, OUT, C), BF16), V((4, OUT, C), BF16),
         V((OUT, D), F32), V((4, OUT, 512), BF16),
-        S((24,)), S((2, 2)), S((2, 2)), S((2, 2)), S((2, 2)), S((2, 3, 2)), S((2, 3, 2)), S((2, 3, 2)), S((2, 3, 2)),
-        S((2, 3, 4)), S((2, 3, 4)),
-        S(()), S(()), S((3,)), S((3,)), S((3,)), S((3,)), S(()), S(()), S(()), S(()), S((3,)), S((3,)), S((3,)), S((3,)),
-        S((4,)),
+        S((17,)), S(()), S((2,)), S((2,)), S((2, 3)), S((2, 3)), S(()),
+        S(()), S(()), S(()), S(()), S((3,)), S((3,)), S(()), S(()), S(()), S(()), S(()), S(()), S(()), S((2,)), S(()),
     ]
 
 

time: 40.3 us -> 39.1 us (0.970)
  Pallas kernels: 39.8 us -> 38.8 us
    pallas_call x1, Pallas kernels: 37.6 us -> 36.6 us  [per_device(): pl.pallas_call(kernel, out_shape=jax.ShapeDtypeStruct((OUT, D), BF16), in...]
where the time goes in v6:
time: 39.1 us; the launch traced here: 39 us
  Pallas kernels  38.8 us (99%)
    pallas_call x1, Pallas kernels, per_device(): pl.pallas_call(kernel, out_shape=jax.ShapeDtypeStruct((OUT, D), BF16), in...  36.6 us
    pallas_call x1, Pallas kernels, per_device(): pl.pallas_call(copy_out, out_shape=jax.ShapeDtypeStruct((OUT, D), BF16),...  2.2 us

profile of v6, /device:TPU:1, one launch (start us, length us, event | category | flops | bytes accessed | tf_op | source)
XLA Modules:
  0.0 39.0 jit_solution(867916926377366689)
XLA Ops:
  0.0 36.6 %shard_map.145.src = bf16[384,2048]{1,0:T(8,128)(2,1)} custom-call(bf16[1536,2048]{1,0:T(8,128)(2,1)} %x_hbm.1, f32[1,2048]{1,0:T(1,128)} %bitcast.6, bf16[2048,256]{1,0:T(8,128)(2,1)} %wp_hbm.1, bf16[2048,256]{1,0:T(8,128)(2,1)} %wq_hbm.1, bf16[2048,256]{1,0:T(8,128)(2,1)} %wf_hbm.1, bf16[2048,256]{1,0:T(8,128)(2,1)} %wv_hbm.1, bf16[2048,256]{1,0:T(8,128)(2,1)} %wg_hbm.1, ...), custom_call_target="tpu_custom_call" | custom-call | tf_op jit(solution)/shard_map/pallas_call | solution.py:598
  36.6 2.2 %shard_map.146 = bf16[384,2048]{1,0:T(8,128)(2,1)} custom-call(bf16[384,2048]{1,0:T(8,128)(2,1)} %shard_map.145.src), custom_call_target="tpu_custom_call" | custom-call | tf_op jit(solution)/shard_map/pallas_call | solution.py:612

commit v7 on v6

--- a/solution.py
+++ b/solution.py
@@ -55,7 +55,7 @@
     totsend, totrecv, ybuf, zbuf, pst, carr, trilb, band,
     ypbuf, ypseen, yrbuf, yrseen, acc, obuf,
     lsem, wsem, w1r, w1fr, w2r, w2fr, w3r,
-    es, er, ys, yr_, zs, zr, cs, cr, hs, hr, aps, apr, ars, arr, osem,
+    es, er, yr_, zs, zr, cr, hs, hr, aps, apr, ars, arr, osem,
 ):
     x = lax.axis_index("tp")
     sp = lax.axis_index("sp")
@@ -417,7 +417,7 @@
     la, lS = jnp.where(first, sa, oa), jnp.where(first, sS, oS)
     put_state(ybuf.at[y], *chain(ea, eS, la, lS))
     for k in (2, 1, 3):
-        remote(ybuf.at[y], ybuf.at[y], ys, yr_, ypeer(k))
+        remote(ybuf.at[y], ybuf.at[y], es, yr_, ypeer(k))
 
     @pl.when(sp < 31)
     def _():
@@ -480,7 +480,7 @@
     l_rg.wait()
     do_proj(1)
     wait_bytes(ybuf.at[pl.ds(0, 3)], yr_)
-    wait_bytes(ybuf.at[pl.ds(0, 3)], ys)
+    wait_bytes(ybuf.at[pl.ds(0, 3)], es)
     ta, tS, ya, yS = scan_states(ybuf, y)
     put_state(zbuf.at[z], ta, tS)
     pst[0:HK, :] = yS
@@ -501,7 +501,7 @@
     l_init.wait()
     fa, fS = chain(za, zS, pst[HK : HK + 1, :], pst[0:HK, :])
     carr[c] = fa * jnp.transpose(init[c]) + fS
-    c_cp = remote(carr.at[c], carr.at[c], cs, cr, sib)
+    c_cp = remote(carr.at[c], carr.at[c], es, cr, sib)
     do_scores(2)
     w2_poll(1, 1)
     w2_poll(1, 0)
@@ -558,16 +558,14 @@
 
 
 def copy_out(src, dst, buf, sin, sout):
-    n = OUT // 4
-    into = [pltpu.make_async_copy(src.at[pl.ds(i * n, n)], buf.at[i], sin.at[i]) for i in range(4)]
-    out = [pltpu.make_async_copy(buf.at[i], dst.at[pl.ds(i * n, n)], sout.at[i]) for i in range(4)]
+    n = OUT // 3
+    into = [pltpu.make_async_copy(src.at[pl.ds(i * n, n)], buf.at[pl.ds(i * n, n)], sin.at[i]) for i in range(3)]
     for cp in into:
         cp.start()
-    for cp, to in zip(into, out):
+    for i, cp in enumerate(into):
         cp.wait()
-        to.start()
-    for to in out:
-        to.wait()
+        pltpu.make_async_copy(buf.at[pl.ds(i * n, n)], dst.at[pl.ds(i * n, n)], sout).start()
+    pltpu.make_async_copy(buf, dst, sout).wait()
 
 
 def scratch():
@@ -585,8 +583,8 @@
         V((BL, BL), BF16), V((BL, 2 * BL), BF16),
         V((3, OUT, C), BF16), V((4, OUT, C), BF16), V((3, OUT, C), BF16), V((4, OUT, C), BF16),
         V((OUT, D), F32), V((4, OUT, 512), BF16),
-        S((17,)), S(()), S((2,)), S((2,)), S((2, 3)), S((2, 3)), S(()),
-        S(()), S(()), S(()), S(()), S((3,)), S((3,)), S(()), S(()), S(()), S(()), S(()), S(()), S(()), S((2,)), S(()),
+        S((16,)), S(()), S((2,)), S((2,)), S((2, 3)), S((2, 3)), S(()),
+        S(()), S(()), S(()), S((3,)), S((3,)), S(()), S(()), S(()), S(()), S(()), S(()), S((2,)), S(()),
     ]
 
 
@@ -615,7 +613,7 @@
         in_specs=[anyspec],
         out_specs=anyspec,
         scratch_shapes=[
-            pltpu.VMEM((4, OUT // 4, D), BF16), pltpu.SemaphoreType.DMA((4,)), pltpu.SemaphoreType.DMA((4,)),
+            pltpu.VMEM((OUT, D), BF16), pltpu.SemaphoreType.DMA((3,)), pltpu.SemaphoreType.DMA(()),
         ],
     )(full)
 

time: 39.1 us -> 39.1 us (level)
  no operation moved by 1% of the time
where the time goes in v7:
time: 39.1 us; the launch traced here: 38.9 us
  Pallas kernels  38.8 us (99%)
    pallas_call x1, Pallas kernels, per_device(): pl.pallas_call(kernel, out_shape=jax.ShapeDtypeStruct((OUT, D), BF16), in...  36.6 us
    pallas_call x1, Pallas kernels, per_device(): pl.pallas_call(copy_out, out_shape=jax.ShapeDtypeStruct((OUT, D), BF16),...  2.21 us

profile of v7, /device:TPU:1, one launch (start us, length us, event | category | flops | bytes accessed | tf_op | source)
XLA Modules:
  0.0 38.9 jit_solution(11554907461845935596)
XLA Ops:
  0.0 36.6 %shard_map.145.src = bf16[384,2048]{1,0:T(8,128)(2,1)} custom-call(bf16[1536,2048]{1,0:T(8,128)(2,1)} %x_hbm.1, f32[1,2048]{1,0:T(1,128)} %bitcast.6, bf16[2048,256]{1,0:T(8,128)(2,1)} %wp_hbm.1, bf16[2048,256]{1,0:T(8,128)(2,1)} %wq_hbm.1, bf16[2048,256]{1,0:T(8,128)(2,1)} %wf_hbm.1, bf16[2048,256]{1,0:T(8,128)(2,1)} %wv_hbm.1, bf16[2048,256]{1,0:T(8,128)(2,1)} %wg_hbm.1, ...), custom_call_target="tpu_custom_call" | custom-call | tf_op jit(solution)/shard_map/pallas_call | solution.py:596
  36.6 2.2 %shard_map.146 = bf16[384,2048]{1,0:T(8,128)(2,1)} custom-call(bf16[384,2048]{1,0:T(8,128)(2,1)} %shard_map.145.src), custom_call_target="tpu_custom_call" | custom-call | tf_op jit(solution)/shard_map/pallas_call | solution.py:610
